TPU v7x, 256 devices: a whole 4x4x8 slice. The times are simulated.
256 devices in a mesh: rep: 2 (over z_hi), fs: 16 (over z_lo, x), tp: 8 (over y, core).
Axes of the slice: x: 4, y: 4, z: 8 (z_hi: 2, z_lo: 4; z = z_hi * 4 + z_lo), core: 2. Of those that a mesh axis runs over, the one named last changes fastest.
Arguments:
- tokens: bfloat16 [32768, 2048], P(('rep', 'fs', 'tp')), may hold values from -6 to 6
- mixer_gain: float32 [2048], replicated, may hold values from 0.1 to 1.9
- direct_weight: float32 [2048, 1024], P('fs', 'tp'), may hold values from -0.125 to 0.125
- direct_scale: float32 [1024], P('tp'), may hold values from 0.5 to 2
- value_weight: float32 [2048, 1024], P('fs', 'tp'), may hold values from -0.125 to 0.125
- value_scale: float32 [1024], P('tp'), may hold values from 0.5 to 8, as said below
- value_gain: float32 [1024], P('tp'), may hold values from 0.1 to 1.9
- value_shift: float32 [1024], P('tp'), may hold values from -3 to 3
- spatial_weight: bfloat16 [16, 128, 128], P('tp'), may hold values from -0.25 to 0.25
- spatial_bias: float32 [16, 128], P('tp'), may hold values from 0.1 to 1.9
- merge_weight: float32 [1024, 2048], P('tp', 'fs'), may hold values from -0.1875 to 0.1875
- merge_scale: float32 [2048], P('fs'), may hold values from 0.5 to 2
- channel_gain: float32 [2048], replicated, may hold values from 0.1 to 1.9
- expand_weight: float32 [2048, 8192], P('fs', 'tp'), may hold values from -0.125 to 0.125
- expand_scale: float32 [8192], P('tp'), may hold values from 0.5 to 2
- reduce_weight: float32 [8192, 2048], P('tp', 'fs'), may hold values from -0.0625 to 0.0625
- reduce_scale: float32 [2048], P('fs'), may hold values from 0.5 to 2
Outputs:
- result: bfloat16 [32768, 2048], P(('rep', 'fs', 'tp'))
Inputs may be any that keep to these rules, and one draw needn't show every extreme that they name: `value_scale`: positive column scales.
All inputs are finite; a program needn't handle non-finite values.
Results may differ from a plain program's by a relative error of at most 0.024.
Values may be sent and summed in bfloat16 or wider, within the bound.
A program may use at most 64 MiB of HBM per device.

v0:
```python
import jax
import jax.numpy as jnp
from jax import lax
from jax.sharding import Mesh
from jax.sharding import PartitionSpec as P

GDIM = 64
BLOCK = 128
TP = ("tp_0", "tp_1")
REP_FS_TP = ("rep", "fs", "tp_0", "tp_1")


epsilon = 1e-06


def copy_for_each(x, axis):
    copies = jnp.broadcast_to(x, (lax.axis_size(axis), *x.shape))
    return lax.all_to_all(copies, axis, split_axis=0, concat_axis=0, tiled=True)


def in_order(blocks, dim):
    lengths = list(blocks.shape[1:])
    lengths[dim] *= blocks.shape[0]
    return jnp.moveaxis(blocks, 0, dim).reshape(lengths)


def gathered_by_axis(x, axes, dim):
    far, near = axes
    blocks = copy_for_each(copy_for_each(x, far), near)
    return in_order(blocks.swapaxes(0, 1).reshape(-1, *x.shape), dim)


def sent_together(arrays, axis, dim, along):
    widths = [a.shape[along] for a in arrays]
    both = jnp.concatenate(arrays, axis=along)
    filled = lax.all_gather(both, axis, axis=dim, tiled=True)
    return tuple(jnp.split(filled, [sum(widths[:k]) for k in range(1, len(widths))], axis=along))


def of_everyone(x, axis):
    everything = copy_for_each(x, axis)
    return jnp.sum(everything, axis=0)


def together(arrays, axis):
    ravelled, at, done = (jnp.concatenate([a.reshape(-1) for a in arrays]), 0, [])
    so_far = of_everyone(ravelled, axis)
    for a in arrays:
        done.append(so_far[at : at + a.size].reshape(a.shape))
        at += a.size
    return tuple(done)


def in_blocks(x, dim, devices):
    lengths = x.shape
    blocks = x.reshape(*lengths[:dim], devices, lengths[dim] // devices, *lengths[dim + 1 :])
    return jnp.moveaxis(blocks, dim, 0)


def sent_and_summed(x, axis, dim):
    blocks = in_blocks(x, dim, lax.axis_size(axis))
    arrived = lax.all_to_all(blocks, axis, split_axis=0, concat_axis=0, tiled=True)
    return arrived.astype(jnp.float32).sum(axis=0)


def sum_in_two_steps(x, axes, dim):
    far, near = axes
    own = sent_and_summed(in_blocks(x, dim, lax.axis_size(far)), near, dim + 1)
    return jnp.sum(
        lax.all_to_all(own.astype(jnp.bfloat16), far, 0, 0, tiled=True).astype(jnp.float32), axis=0
    )


def rms_rows(rows, gain):
    floats = rows.astype(jnp.float32)
    scaled = floats * lax.rsqrt(jnp.mean(floats * floats, axis=-1, keepdims=True) + epsilon)
    return (scaled * gain).astype(jnp.bfloat16)


def body(
    tokens,
    mixer_gain,
    direct_weight,
    direct_scale,
    value_weight,
    value_scale,
    value_gain,
    value_shift,
    spatial_weight,
    spatial_bias,
    merge_weight,
    merge_scale,
    channel_gain,
    expand_weight,
    expand_scale,
    reduce_weight,
    reduce_scale,
):
    direct_half = direct_weight.astype(jnp.bfloat16)
    value_half = value_weight.astype(jnp.bfloat16)
    merge_half = merge_weight.astype(jnp.bfloat16)
    expand_half = expand_weight.astype(jnp.bfloat16)
    reduce_half = reduce_weight.astype(jnp.bfloat16)
    full_expand, full_reduce, reduce_full_scale = (
        lax.all_gather(expand_half, "fs", axis=0, tiled=True),
        lax.all_gather(reduce_half, "fs", axis=1, tiled=True),
        lax.all_gather(reduce_scale.astype(jnp.bfloat16), "fs", axis=0, tiled=True).astype(
            reduce_scale.dtype
        ),
    )
    normed = rms_rows(tokens, mixer_gain)
    whole = gathered_by_axis(normed, ("tp_0", "tp_1"), 0)
    seq_rows = whole.shape[0]
    local_width = direct_weight.shape[1]
    full_direct, full_value, full_merge, merge_full_scale = (
        *sent_together((direct_half, value_half), "fs", 0, 1),
        lax.all_gather(merge_half, "fs", axis=1, tiled=True),
        lax.all_gather(merge_scale.astype(jnp.bfloat16), "fs", axis=0, tiled=True).astype(
            merge_scale.dtype
        ),
    )
    direct_pre = jnp.dot(whole, full_direct, preferred_element_type=jnp.float32)
    value_pre = jnp.dot(whole, full_value, preferred_element_type=jnp.float32)
    direct = jax.nn.gelu(direct_pre * direct_scale)
    value = jax.nn.gelu(value_pre * value_scale)
    total, squares = together((jnp.sum(value, axis=1), jnp.sum(value * value, axis=1)), TP)
    branch_width = local_width * lax.axis_size(TP)
    mean = (total / branch_width)[:, None]
    var = (squares / branch_width)[:, None] - mean * mean
    gated_value = ((value - mean) * lax.rsqrt(var + epsilon) * value_gain + value_shift).astype(
        jnp.bfloat16
    )
    local_groups = spatial_weight.shape[0]
    blocks = gated_value.reshape(seq_rows // BLOCK, BLOCK, local_groups, GDIM)
    mixed = jnp.einsum("gpq,nqgc->npgc", spatial_weight, blocks, preferred_element_type=jnp.float32)
    mixed = mixed + jnp.transpose(spatial_bias)[None, :, :, None]
    gated = (direct * mixed.reshape(seq_rows, local_width)).astype(jnp.bfloat16)
    rows = gated
    mix = sum_in_two_steps(
        (jnp.dot(rows, full_merge, preferred_element_type=jnp.float32) * merge_full_scale).astype(
            jnp.bfloat16
        ),
        ("tp_0", "tp_1"),
        0,
    )
    middle = (tokens.astype(jnp.float32) + mix).astype(jnp.bfloat16)
    normed_mid = rms_rows(middle, channel_gain)
    whole_mid = gathered_by_axis(normed_mid, ("tp_0", "tp_1"), 0)
    upper = jnp.dot(whole_mid, full_expand, preferred_element_type=jnp.float32)
    hidden = jnp.square(jax.nn.relu(upper * expand_scale)).astype(jnp.bfloat16)
    rows = hidden
    lower = sum_in_two_steps(
        (jnp.dot(rows, full_reduce, preferred_element_type=jnp.float32) * reduce_full_scale).astype(
            jnp.bfloat16
        ),
        ("tp_0", "tp_1"),
        0,
    )
    return (middle.astype(jnp.float32) + lower).astype(jnp.bfloat16)


def solution(mesh):
    finer = Mesh(
        mesh.devices.reshape(mesh.shape["rep"], mesh.shape["fs"], 4, 2),
        ("rep", "fs", "tp_0", "tp_1"),
    )
    in_specs = (
        P(REP_FS_TP, None),
        P(),
        P("fs", TP),
        P(TP),
        P("fs", TP),
        P(TP),
        P(TP),
        P(TP),
        P(TP, None, None),
        P(TP, None),
        P(TP, "fs"),
        P("fs"),
        P(),
        P("fs", TP),
        P(TP),
        P(TP, "fs"),
        P("fs"),
    )
    out_specs = P(REP_FS_TP, None)
    return jax.shard_map(body, mesh=finer, in_specs=in_specs, out_specs=out_specs, check_vma=False)
```

profile of v0, /device:TPU:1, one launch (start us, length us, event | category | flops | bytes accessed | tf_op | source)
XLA Modules:
  0.0 337.2 jit_solution(3194042908700379348)
XLA Ops:
  9.0 1.8 convert_element_type.88
  14.9 5.0 %all-to-all-start = ((bf16[4,128,2048]{2,1,0:T(8,128)(2,1)}), bf16[4,128,2048]{2,1,0:T(8,128)(2,1)S(1)}, u32[]{:S(2)}, u32[]{:S(2)}) async-start(bf16[4,128,2048]{2,1,0:T(8,128)(2,1)} %broadcast_in_dim.10), calls=%async_computation | async-start | bytes 4194304 | tf_op jit(solution)/shard_map/all_to_all | solution.py:18
  20.7 40.5 %all_gather.19 = bf16[128,2048]{1,0:T(8,128)(2,1)S(1)} all-gather(bf16[128,128]{1,0:T(8,128)(2,1)S(1)} %convert_element_type.78), channel_id=1, replica_groups=mesh['rep'=2,'fs'=16,'tp_0'=4,'tp_1'=2] {'fs'}, dimensions={1}, use_global_device_ids=true | all-gather | bytes 557056 | tf_op jit(solution)/shard_map/all_gather | solution.py:117
  61.7 13.7 %all_to_all.46 = bf16[2,4,128,2048]{3,2,1,0:T(8,128)(2,1)S(1)} all-to-all(bf16[2,4,128,2048]{3,2,1,0:T(8,128)(2,1)S(1)} %broadcast_in_dim.11), channel_id=1, replica_groups=mesh['rep'=2,'fs'=16,'tp_0'=4,'tp_1'=2] {'tp_1'}, dimensions={0} | all-to-all | bytes 8388608 | tf_op jit(solution)/shard_map/all_to_all | solution.py:18
  75.4 2.3 copy.44
  77.7 5.5 %all-gather.6.cloned.1.call-done = bf16[2048,256]{1,0:T(8,128)(2,1)} async-done(((bf16[128,256]{1,0:T(8,128)(2,1)}), bf16[2048,256]{1,0:T(8,128)(2,1)}) %all-gather.6.cloned.1.call-update) | async-done | bytes 1048592 | tf_op jit(solution)/shard_map/all_gather | solution.py:36
  83.2 3.7 %fusion.43 = (f32[1024]{0:T(1024)S(1)}, f32[1024]{0:T(1024)S(1)}, f32[1024,128]{1,0:T(8,128)S(1)}) fusion(f32[128]{0:T(128)S(1)} %copy-done.10, bf16[1024,2048]{1,0:T(8,128)(2,1)} %bitcast.38, bf16[2048,256]{1,0:T(8,128)(2,1)} %all-gather.6.cloned.1.call-done), kind=kOutput, calls=%fused_computation.70 | convolution fusion | flops 538441728 | bytes 5251584 | tf_op jit(solution)/shard_map/dot_general | solution.py:123
  87.6 15.7 %all-to-all-start.2 = ((f32[8,1,2048]{2,1,0:T(1,128)}), f32[8,1,2048]{2,1,0:T(1,128)S(1)}, u32[]{:S(2)}, u32[]{:S(2)}) async-start(f32[8,1,2048]{2,1,0:T(1,128)} %broadcast_in_dim.12), calls=%async_computation.2 | async-start | bytes 131072 | tf_op jit(solution)/shard_map/all_to_all | solution.py:18
  103.3 35.4 %all-gather = bf16[16,1,128]{2,1,0:T(2,128)(2,1)S(1)} all-gather(bf16[1,1,128]{2,1,0:T(2,128)(2,1)S(1)} %convert_bitcast_fusion.1), channel_id=1, replica_groups=mesh['rep'=2,'fs'=16,'tp_0'=4,'tp_1'=2] {'fs'}, dimensions={0}, use_global_device_ids=true | all-gather | bytes 4352 | tf_op jit(solution)/shard_map/all_gather | solution.py:118
  141.0 8.6 %multiply_convert_fusion.1 = bf16[1024,2048]{1,0:T(8,128)(2,1)} fusion(bf16[128,2048]{1,0:T(8,128)(2,1)S(1)} %all_gather.19, f32[2048]{0:T(1024)S(1)} %bitcast.43, f32[1024,128]{1,0:T(8,128)S(1)} %reshape.52, bf16[1024,2048]{1,0:T(8,128)(2,1)} %bitcast.39, bf16[2048,256]{1,0:T(8,128)(2,1)} %all-gather.6.cloned.1.call-done, f32[128]{0:T(128)S(1)} %copy-done.12), kind=kOutput, calls=%fused_computation.1 | convolution fusion | flops 1079377920 | bytes 9970176 | tf_op jit(solution)/shard_map/dot_general | solution.py:140
  149.6 2.5 copy.68
  152.2 14.0 %all_to_all.47 = bf16[2,4,128,2048]{3,2,1,0:T(8,128)(2,1)} all-to-all(bf16[2,4,128,2048]{3,2,1,0:T(8,128)(2,1)S(1)} %bitcast.36), channel_id=1, replica_groups=mesh['rep'=2,'fs'=16,'tp_0'=4,'tp_1'=2] {'tp_1'}, dimensions={0} | all-to-all | bytes 8388608 | tf_op jit(solution)/shard_map/all_to_all | solution.py:62
  166.1 3.5 %reduce_sum.91 = bf16[4,128,2048]{2,1,0:T(8,128)(2,1)S(1)} reduce(bf16[2,4,128,2048]{3,2,1,0:T(8,128)(2,1)} %all_to_all.47, bf16[]{:T(256)} %constant.25.clone.1), dimensions={0}, to_apply=%region_4.0 | reduce | flops 1048576 | bytes 6291458 | tf_op jit(solution)/shard_map/reduce_sum | solution.py:63
  169.7 29.9 %all_to_all.48 = bf16[4,128,2048]{2,1,0:T(8,128)(2,1)S(1)} all-to-all(bf16[4,128,2048]{2,1,0:T(8,128)(2,1)S(1)} %reduce_sum.91), channel_id=1, replica_groups=mesh['rep'=2,'fs'=16,'tp_0'=4,'tp_1'=2] {'tp_0'}, dimensions={0} | all-to-all | bytes 4194304 | tf_op jit(solution)/shard_map/all_to_all | solution.py:70
  202.1 3.6 %all-to-all-start.5 = ((bf16[4,128,2048]{2,1,0:T(8,128)(2,1)}), bf16[4,128,2048]{2,1,0:T(8,128)(2,1)S(1)}, u32[]{:S(2)}, u32[]{:S(2)}) async-start(bf16[4,128,2048]{2,1,0:T(8,128)(2,1)} %broadcast_in_dim.13), calls=%async_computation.5 | async-start | bytes 4194304 | tf_op jit(solution)/shard_map/all_to_all | solution.py:18
  205.8 31.6 %all-gather.1 = bf16[16,1,128]{2,1,0:T(2,128)(2,1)S(1)} all-gather(bf16[1,1,128]{2,1,0:T(2,128)(2,1)S(1)} %convert_bitcast_fusion), channel_id=1, replica_groups=mesh['rep'=2,'fs'=16,'tp_0'=4,'tp_1'=2] {'fs'}, dimensions={0}, use_global_device_ids=true | all-gather | bytes 4352 | tf_op jit(solution)/shard_map/all_gather | solution.py:107
  237.9 13.7 %all_to_all.49 = bf16[2,4,128,2048]{3,2,1,0:T(8,128)(2,1)S(1)} all-to-all(bf16[2,4,128,2048]{3,2,1,0:T(8,128)(2,1)S(1)} %broadcast_in_dim.14), channel_id=1, replica_groups=mesh['rep'=2,'fs'=16,'tp_0'=4,'tp_1'=2] {'tp_1'}, dimensions={0} | all-to-all | bytes 8388608 | tf_op jit(solution)/shard_map/all_to_all | solution.py:18
  251.7 2.3 copy.52
  253.9 8.5 %all-gather.8.cloned.1.call-done = bf16[2048,1024]{1,0:T(8,128)(2,1)} async-done(((bf16[128,1024]{1,0:T(8,128)(2,1)}), bf16[2048,1024]{1,0:T(8,128)(2,1)}) %all-gather.8.cloned.1.call-update) | async-done | bytes 4194320 | tf_op jit(solution)/shard_map/all_gather | solution.py:105
  262.5 14.4 %multiply_convert_fusion = bf16[1024,2048]{1,0:T(8,128)(2,1)} fusion(bf16[1024,2048]{1,0:T(8,128)(2,1)} %all-gather.10.cloned.1.call-done, f32[2048]{0:T(1024)S(1)} %bitcast.44, bf16[1024,2048]{1,0:T(8,128)(2,1)} %bitcast.40, bf16[2048,1024]{1,0:T(8,128)(2,1)} %all-gather.8.cloned.1.call-done, f32[1024]{0:T(1024)S(1)} %copy-done.9), kind=kOutput, calls=%fused_computation | convolution fusion | flops 8598323200 | bytes 16789504 | tf_op jit(solution)/shard_map/dot_general | solution.py:153
  276.8 2.5 copy.67
  279.3 17.1 %all_to_all.50 = bf16[2,4,128,2048]{3,2,1,0:T(8,128)(2,1)} all-to-all(bf16[2,4,128,2048]{3,2,1,0:T(8,128)(2,1)S(1)} %bitcast.37), channel_id=1, replica_groups=mesh['rep'=2,'fs'=16,'tp_0'=4,'tp_1'=2] {'tp_1'}, dimensions={0} | all-to-all | bytes 8388608 | tf_op jit(solution)/shard_map/all_to_all | solution.py:62
  296.5 3.6 %reduce_sum.94 = bf16[4,128,2048]{2,1,0:T(8,128)(2,1)S(1)} reduce(bf16[2,4,128,2048]{3,2,1,0:T(8,128)(2,1)} %all_to_all.50, bf16[]{:T(256)} %constant.25.clone.1), dimensions={0}, to_apply=%region_7.8 | reduce | flops 1048576 | bytes 6291458 | tf_op jit(solution)/shard_map/reduce_sum | solution.py:63
  300.0 29.3 %all_to_all.51 = bf16[4,128,2048]{2,1,0:T(8,128)(2,1)S(1)} all-to-all(bf16[4,128,2048]{2,1,0:T(8,128)(2,1)S(1)} %reduce_sum.94), channel_id=1, replica_groups=mesh['rep'=2,'fs'=16,'tp_0'=4,'tp_1'=2] {'tp_0'}, dimensions={0} | all-to-all | bytes 4194304 | tf_op jit(solution)/shard_map/all_to_all | solution.py:70
  (69 shorter events, 15.0 us)
Async XLA Ops:
  6.5 132.9 %copy-start = (bf16[2,128,128]{2,1,0:T(8,128)(2,1)S(1)}, bf16[2,128,128]{2,1,0:T(8,128)(2,1)}, u32[]{:S(2)}) copy-start(bf16[2,128,128]{2,1,0:T(8,128)(2,1)} %param.25) | copy-start | bytes 196612
  6.5 76.7 %all-gather.6.cloned.1.call-start = ((), (), s32[]{:S(2)}) async-start(), calls=%async_computation.9 | async-start | bytes 1114112 | tf_op jit(solution)/shard_map/all_gather | solution.py:36
  8.9 245.0 %all-gather.10.cloned.1.call-start = ((), (), s32[]{:S(2)}) async-start(), calls=%async_computation.11 | async-start | bytes 4456448 | tf_op jit(solution)/shard_map/all_gather | solution.py:106
  10.8 9.2 %copy-start.3 = (f32[128,1024]{1,0:T(8,128)S(1)}, f32[128,1024]{1,0:T(8,128)}, u32[]{:S(2)}) copy-start(f32[128,1024]{1,0:T(8,128)} %param.30) | copy-start | bytes 1572868
  13.3 7.4 %copy-start.4 = (f32[128,128]{1,0:T(8,128)S(1)}, f32[128,128]{1,0:T(8,128)}, u32[]{:S(2)}) copy-start(f32[128,128]{1,0:T(8,128)} %param.27) | copy-start | bytes 196612
  14.9 46.3 %all-to-all-start = ((bf16[4,128,2048]{2,1,0:T(8,128)(2,1)}), bf16[4,128,2048]{2,1,0:T(8,128)(2,1)S(1)}, u32[]{:S(2)}, u32[]{:S(2)}) async-start(bf16[4,128,2048]{2,1,0:T(8,128)(2,1)} %broadcast_in_dim.10), calls=%async_computation | async-start | bytes 4194304 | tf_op jit(solution)/shard_map/all_to_all | solution.py:18
  19.9 242.5 %all-gather.8.cloned.1.call-start = ((), (), s32[]{:S(2)}) async-start(), calls=%async_computation.10 | async-start | bytes 4456448 | tf_op jit(solution)/shard_map/all_gather | solution.py:105
  75.4 7.8 %copy-start.10 = (f32[128]{0:T(128)S(1)}, f32[128]{0:T(128)}, u32[]{:S(2)}) copy-start(f32[128]{0:T(128)} %param.22) | copy-start | bytes 1540
  83.2 20.1 %copy-start.11 = (f32[128]{0:T(128)S(1)}, f32[128]{0:T(128)}, u32[]{:S(2)}) copy-start(f32[128]{0:T(128)} %param.28) | copy-start | bytes 1540
  83.2 55.6 %copy-start.7 = (f32[128]{0:T(128)S(1)}, f32[128]{0:T(128)}, u32[]{:S(2)}) copy-start(f32[128]{0:T(128)} %param.24) | copy-start | bytes 1540
  83.2 55.6 %copy-start.8 = (f32[128]{0:T(128)S(1)}, f32[128]{0:T(128)}, u32[]{:S(2)}) copy-start(f32[128]{0:T(128)} %param.23) | copy-start | bytes 1540
  83.2 56.3 %copy-start.6 = (f32[2,128]{1,0:T(2,128)S(1)}, f32[2,128]{1,0:T(2,128)}, u32[]{:S(2)}) copy-start(f32[2,128]{1,0:T(2,128)} %param.26) | copy-start | bytes 3076
  87.0 54.1 %copy-start.12 = (f32[128]{0:T(128)S(1)}, f32[128]{0:T(128)}, u32[]{:S(2)}) copy-start(f32[128]{0:T(128)} %param.20) | copy-start | bytes 1540
  87.6 51.1 %all-to-all-start.2 = ((f32[8,1,2048]{2,1,0:T(1,128)}), f32[8,1,2048]{2,1,0:T(1,128)S(1)}, u32[]{:S(2)}, u32[]{:S(2)}) async-start(f32[8,1,2048]{2,1,0:T(1,128)} %broadcast_in_dim.12), calls=%async_computation.2 | async-start | bytes 131072 | tf_op jit(solution)/shard_map/all_to_all | solution.py:18
  169.7 30.3 %copy-start.2 = (bf16[128,2048]{1,0:T(8,128)(2,1)S(1)}, bf16[128,2048]{1,0:T(8,128)(2,1)}, u32[]{:S(2)}) copy-start(bf16[128,2048]{1,0:T(8,128)(2,1)} %param.17) | copy-start | bytes 1572868
  169.7 30.6 %copy-start.5 = (f32[2048]{0:T(1024)S(1)}, f32[2048]{0:T(1024)}, u32[]{:S(2)}) copy-start(f32[2048]{0:T(1024)} %param.29) | copy-start | bytes 24580
  200.3 5.5 %copy-start.13 = (f32[128]{0:T(128)S(1)}, f32[128]{0:T(128)}, u32[]{:S(2)}) copy-start(f32[128]{0:T(128)} %param.33) | copy-start | bytes 1540
  202.1 35.3 %all-to-all-start.5 = ((bf16[4,128,2048]{2,1,0:T(8,128)(2,1)}), bf16[4,128,2048]{2,1,0:T(8,128)(2,1)S(1)}, u32[]{:S(2)}, u32[]{:S(2)}) async-start(bf16[4,128,2048]{2,1,0:T(8,128)(2,1)} %broadcast_in_dim.13), calls=%async_computation.5 | async-start | bytes 4194304 | tf_op jit(solution)/shard_map/all_to_all | solution.py:18
  251.7 10.8 %copy-start.9 = (f32[1024]{0:T(1024)S(1)}, f32[1024]{0:T(1024)}, u32[]{:S(2)}) copy-start(f32[1024]{0:T(1024)} %param.31) | copy-start | bytes 12292
  296.5 34.3 %copy-start.1 = (bf16[2,128,128]{2,1,0:T(8,128)(2,1)S(1)}, bf16[2,128,128]{2,1,0:T(8,128)(2,1)}, u32[]{:S(2)}) copy-start(bf16[2,128,128]{2,1,0:T(8,128)(2,1)} %param.25) | copy-start | bytes 196612
Sparse Core Ops, SparseCore 0:
  9.1 74.0 all-gather.5
  84.9 88.4 all-gather.9
  175.3 87.1 all-gather.7
where the time goes:
time: 339 us; the launch traced here: 337 us
  blocking collectives  225 us (66%)
  matrix products  27 us (8%)
  starting transfers between devices  24.4 us (7%)
  other arithmetic  17.1 us (5%)
  local copies, waits for them, and re-layouts  16 us (5%)
  waiting for transfers between devices  14.1 us (4%)
  between operations  13.4 us (4%)
    all_to_all x2, blocking collectives, sum_in_two_steps(): lax.all_to_all(own.astype(jnp.bfloat16), far, 0, 0, tiled=True)  59.3 us
    all_gather x1, blocking collectives, body(): lax.all_gather(merge_half, 'fs', axis=1, tiled=True)  40.5 us
    all_gather x1, blocking collectives, body(): lax.all_gather(merge_scale.astype(jnp.bfloat16), 'fs', axis=0, tiled=True)  35.4 us
    all_gather x1, blocking collectives, body(): lax.all_gather(reduce_scale.astype(jnp.bfloat16), 'fs', axis=0, tiled=True)  31.6 us
    all_to_all x2, blocking collectives, sent_and_summed(): lax.all_to_all(blocks, axis, split_axis=0, concat_axis=0, tiled=True)  31.1 us
    all_to_all x2, blocking collectives, copy_for_each(): return lax.all_to_all(copies, axis, split_axis=0, concat_axis=0, tiled=True)  27.4 us
    all_to_all x3, starting transfers between devices, copy_for_each(): return lax.all_to_all(copies, axis, split_axis=0, concat_axis=0, tiled=True)  24.3 us
    dot_general x1, matrix products, body(): jnp.dot(rows, full_reduce, preferred_element_type=jnp.float32)  14.4 us
  transfers between devices with their start and end apart: 6, of which 2 were waited for; matrix products, arithmetic and copies ran while one was open for 11% of the time, Pallas kernels for 0%

commit v1 on v0

v1 whole, which is shorter than its diff:
```python
import functools

import jax
import jax.numpy as jnp
from jax import lax
from jax.experimental import pallas as pl
from jax.experimental.pallas import tpu as pltpu
from jax.sharding import Mesh
from jax.sharding import PartitionSpec as P

AXES = ("zh", "zl", "x", "y", "c")
FS = ("zl", "x")
TP = ("y", "c")
EPS = 1e-6
MESH = pl.DeviceIdType.MESH
F32 = jnp.float32
BF16 = jnp.bfloat16

D = 2048
R = 128
CW = 128
HW = 1024
BRANCH = 1024
SP, SN, SF, SO = 0, 1, 2, 3
CHUNK = 32
ORDER = (0, 64, 32, 96)


def gelu(u):
    return jax.nn.gelu(u, approximate=True)


class Gather:
    def __init__(self, view, a, b, pa, pb, sib, send, send_d2d, recv_a, recv_b, recv_d2d):
        self.view, self.a, self.b, self.sib = view, a, b, sib
        self.pa, self.pb = pa, pb
        self.send, self.send_d2d = send, send_d2d
        self.recv_a, self.recv_b, self.recv_d2d = recv_a, recv_b, recv_d2d

    def item(self, da, db, half=None):
        return self.view(lax.rem(self.pa + 4 - da, 4), lax.rem(self.pb + 4 - db, 4), half)

    def copy(self, ref, sem, to):
        return pltpu.make_async_remote_copy(
            src_ref=ref, dst_ref=ref, send_sem=self.send, recv_sem=sem, device_id=to, device_id_type=MESH
        )

    def along_b(self, da):
        ref = self.item(da, 0)
        self.copy(ref, self.recv_b.at[da, 0], self.b[0]).start()
        self.copy(ref, self.recv_b.at[da, 1], self.b[1]).start()

    def across(self, da, db):
        ref = self.item(da, db)
        pltpu.make_async_remote_copy(
            src_ref=ref,
            dst_ref=ref,
            send_sem=self.send_d2d,
            recv_sem=self.recv_d2d,
            device_id=self.sib,
            device_id_type=MESH,
        ).start()

    def landed(self, ref, sem):
        self.copy(ref, sem, self.sib).wait_recv()

    def near_a(self, k):
        da = (1, 3)[k]
        self.landed(self.item(da, 0), self.recv_a.at[k])
        self.copy(self.item(da, 0, k), self.recv_a.at[2 + k], self.a[k]).start()
        self.along_b(da)
        self.across(da, 0)

    def near_b(self, da):
        for k in range(2):
            db = (1, 3)[k]
            self.landed(self.item(da, db), self.recv_b.at[da, k])
            self.copy(self.item(da, db, k), self.recv_b.at[da, 2 + k], self.b[k]).start()
            self.across(da, db)

    def far_b(self, da):
        for k in range(2):
            self.landed(self.item(da, 2, k), self.recv_b.at[da, 2 + k])
        self.across(da, 2)

    def wave0(self):
        ref = self.item(0, 0)
        for k in range(2):
            self.copy(ref, self.recv_a.at[k], self.a[k]).start()
        self.along_b(0)
        self.across(0, 0)

    def wave1(self):
        for k in range(2):
            self.near_a(k)
        self.near_b(0)

    def wave2(self):
        for k in range(2):
            self.landed(self.item(2, 0, k), self.recv_a.at[2 + k])
        self.along_b(2)
        self.across(2, 0)
        self.near_b(1)
        self.near_b(3)
        self.far_b(0)

    def wave3(self):
        self.near_b(2)
        self.far_b(1)
        self.far_b(3)

    def wave4(self):
        self.far_b(2)


def kernel(
    tokens,
    mixer_gain,
    direct_weight,
    direct_scale,
    value_weight,
    value_scale,
    value_gain,
    value_shift,
    spatial_weight,
    spatial_bias,
    merge_weight,
    merge_scale,
    channel_gain,
    expand_weight,
    expand_scale,
    reduce_weight,
    reduce_scale,
    out,
    mixw,
    we,
    wr,
    xbuf,
    x2buf,
    part1,
    part2,
    rel,
    near,
    mrg,
    hbuf,
    dbuf,
    vbuf,
    gbuf,
    rbuf,
    stat,
    small,
    swb,
    bias,
    in_sem,
    ag_send,
    ag_recv,
    rs_send,
    rs_recv,
    st_send,
    st_recv,
    sm_send,
    sm_recv,
    w_send,
    w_send_d2d,
    w_recv_a,
    w_recv_b,
    w_recv_d2d,
):
    zh, zl, x, y, c = (lax.axis_index(name) for name in AXES)
    z = zh * 4 + zl
    fs = zl * 4 + x
    other = 1 - c

    def at_z(w):
        w = lax.rem(w, 8)
        return {"zh": lax.div(w, 4), "zl": lax.rem(w, 4)}

    xs = ({"x": lax.rem(x + 1, 4)}, {"x": lax.rem(x + 3, 4)})
    zs = (at_z(z + 1), at_z(z + 7))
    ynext, yprev, yfar = ({"y": lax.rem(y + k, 4)} for k in (1, 3, 2))
    sib = {"c": other}

    own_rows = pl.ds(SO * R, R)
    pltpu.make_async_copy(tokens, xbuf.at[own_rows], in_sem).start()

    barrier = pltpu.get_barrier_semaphore()
    for to in (*xs, *zs, ynext, yprev, yfar, sib):
        pl.semaphore_signal(barrier, inc=1, device_id=to, device_id_type=MESH)
    pl.semaphore_wait(barrier, 8)

    def rcopy(src, dst, ssem, rsem, to):
        return pltpu.make_async_remote_copy(
            src_ref=src, dst_ref=dst, send_sem=ssem, recv_sem=rsem, device_id=to, device_id_type=MESH
        )

    def gather_copy(buf, phase, way, k):
        if k < 4:
            src = buf.at[pl.ds(SO * R + ORDER[k], CHUNK)]
            dst = buf.at[pl.ds((SP, SN)[way] * R + ORDER[k], CHUNK)]
        else:
            row = 64 * way + CHUNK * (k - 4)
            src = buf.at[pl.ds((SP, SN)[way] * R + row, CHUNK)]
            dst = buf.at[pl.ds(SF * R + row, CHUNK)]
        return rcopy(
            src, dst, ag_send.at[phase, way, k], ag_recv.at[phase, way, k], (ynext, yprev)[way]
        )

    def gather_pass_on(buf, phase):
        for k in range(2):
            for way in range(2):
                chunk = ORDER.index(64 * way + CHUNK * k)
                gather_copy(buf, phase, way, chunk).wait_recv()
                gather_copy(buf, phase, way, 4 + k).start()

    def gather_near(buf, phase):
        for way in range(2):
            for k in range(4):
                if ORDER[k] // 64 != way:
                    gather_copy(buf, phase, way, k).wait_recv()

    def gather_far(buf, phase):
        for way in range(2):
            for k in range(2):
                gather_copy(buf, phase, way, 4 + k).wait_recv()

    def scatter_own(part, phase, way):
        rows = pl.ds(64 * (1 - way), 64)
        src = part.at[pl.ds((SN, SP)[way] * R + 64 * (1 - way), 64)]
        return rcopy(
            src,
            near.at[phase, way, rows],
            rs_send.at[phase, way, 0],
            rs_recv.at[phase, way, 0],
            (ynext, yprev)[way],
        )

    def scatter_far(part, phase, way, k):
        row = CHUNK * k
        return rcopy(
            part.at[pl.ds(SF * R + 64 * way + row, CHUNK)],
            rel.at[phase, way, pl.ds(row, CHUNK)],
            rs_send.at[phase, way, 1 + k],
            rs_recv.at[phase, way, 1 + k],
            (ynext, yprev)[way],
        )

    def scatter_joined(phase, way, k):
        row = CHUNK * k
        return rcopy(
            mrg.at[phase, way, pl.ds(row, CHUNK)],
            near.at[phase, way, pl.ds(64 * way + row, CHUNK)],
            rs_send.at[phase, way, 3 + k],
            rs_recv.at[phase, way, 3 + k],
            (ynext, yprev)[way],
        )

    def scatter_join(part, phase):
        for k in range(2):
            for way in range(2):
                row = CHUNK * k
                scatter_far(part, phase, way, k).wait_recv()
                mine = part[pl.ds((SN, SP)[way] * R + 64 * way + row, CHUNK), :].astype(F32)
                came = rel[phase, way, pl.ds(row, CHUNK), :].astype(F32)
                mrg[phase, way, pl.ds(row, CHUNK), :] = (mine + came).astype(BF16)
                scatter_joined(phase, way, k).start()

    def scatter_finish(part, phase, base, done):
        for way in range(2):
            scatter_own(part, phase, way).wait_recv()
        for k in range(2):
            for way in range(2):
                scatter_joined(phase, way, k).wait_recv()
                row = 64 * way + CHUNK * k
                total = part[pl.ds(SO * R + row, CHUNK), :].astype(F32)
                total = total + near[phase, 0, pl.ds(row, CHUNK), :].astype(F32)
                total = total + near[phase, 1, pl.ds(row, CHUNK), :].astype(F32)
                mine = base[pl.ds(SO * R + row, CHUNK), :].astype(F32)
                done(row, (mine + total).astype(BF16))

    def view_mix(low):
        def view(pz, px, half):
            row = (pz * 4 + px) * 128 + low
            if half is None:
                return mixw.at[c, pl.ds(pl.multiple_of(row, 64), 64)]
            return mixw.at[c, pl.ds(pl.multiple_of(row + 32 * half, 32), 32)]

        return view

    def view_expand(pz, px, half):
        row = (pz * 4 + px) * 128
        if half is None:
            return we.at[c, pl.ds(pl.multiple_of(row, 128), 128)]
        return we.at[c, pl.ds(pl.multiple_of(row + 64 * half, 64), 64)]

    def view_reduce(pz, px, half):
        row = c * HW
        if half is None:
            return wr.at[pz * 4 + px, pl.ds(pl.multiple_of(row, HW), HW)]
        return wr.at[pz * 4 + px, pl.ds(pl.multiple_of(row + 512 * half, 512), 512)]

    def weight(index, view, x_first):
        if x_first:
            a, b, pa, pb, turned = xs, zs, x, zl, lambda p, q, h: view(q, p, h)
        else:
            a, b, pa, pb, turned = zs, xs, zl, x, view
        return Gather(
            turned,
            a,
            b,
            pa,
            pb,
            sib,
            w_send.at[index],
            w_send_d2d.at[index],
            w_recv_a.at[index],
            w_recv_b.at[index],
            w_recv_d2d.at[index],
        )

    mix_a = weight(0, view_mix(0), True)
    mix_b = weight(1, view_mix(64), False)
    expand = weight(2, view_expand, True)
    reduce = weight(3, view_reduce, False)

    def column(row):
        return jnp.transpose(jnp.broadcast_to(row, (128, 128)))

    pltpu.make_async_copy(tokens, xbuf.at[own_rows], in_sem).wait()
    for k in range(4):
        for way in range(2):
            gather_copy(xbuf, 0, way, k).start()

    fs_row = pl.ds(pl.multiple_of(fs * 128, 128), 128)
    gain = column(mixer_gain[pl.ds(fs, 1), :])
    mixw[c, fs_row, 0:128] = (direct_weight[...] * gain * direct_scale[...]).astype(BF16)
    mixw[c, fs_row, 128:256] = (value_weight[...] * gain * value_scale[...]).astype(BF16)
    mixw[c, fs_row, 256:384] = (merge_weight[...] * merge_scale[...]).astype(BF16)
    mix_a.wave0()
    mix_b.wave0()
    small[c, 0:1, :] = value_gain[...]
    small[c, 1:2, :] = value_shift[...]
    small[c, 2:4, :] = spatial_bias[...]
    small[c, 4:8, :] = jnp.zeros((4, 128), F32)
    swb[c] = spatial_weight[...]
    small_copy = rcopy(small.at[c], small.at[c], sm_send.at[0], sm_recv.at[0], sib)
    spatial_copy = rcopy(spatial_weight, swb.at[c], sm_send.at[1], sm_recv.at[1], sib)
    small_copy.start()
    spatial_copy.start()

    gain = column(channel_gain[pl.ds(fs, 1), :])
    for k in range(8):
        lanes = slice(k * 128, (k + 1) * 128)
        we[c, fs_row, lanes] = (expand_weight[:, lanes] * gain * expand_scale[:, lanes]).astype(BF16)
    for k in range(8):
        rows = pl.ds(pl.multiple_of(c * HW + k * 128, 128), 128)
        wr[fs, rows, :] = (reduce_weight[k * 128 : (k + 1) * 128, :] * reduce_scale[...]).astype(BF16)

    mix_a.wave1()
    mix_b.wave1()
    mix_a.wave2()
    mix_b.wave2()
    gather_pass_on(xbuf, 0)
    mix_a.wave3()
    mix_b.wave3()
    expand.wave0()
    reduce.wave0()
    mix_a.wave4()
    mix_b.wave4()

    def row_scales(buf, pair):
        @pl.loop(0, 8)
        def _(i):
            rows = pl.ds(pl.multiple_of(pair * 256 + i * 32, 32), 32)
            floats = buf[rows, :].astype(F32)
            power = jnp.mean(floats * floats, axis=-1, keepdims=True)
            rbuf[rows, :] = jnp.broadcast_to(lax.rsqrt(power + EPS), (32, 128))

    lane = lax.broadcasted_iota(jnp.int32, (128, 128), 1)
    block_of = {SP: lax.rem(y + 3, 4), SN: lax.rem(y + 1, 4), SF: lax.rem(y + 2, 4), SO: y}

    def project(pair):
        row_scales(xbuf, pair)
        for s in range(2):
            rows = pl.ds(pair * 256, 256)
            scale = rbuf[rows, :]
            both = jnp.dot(xbuf[rows, :], mixw[s, :, 0:256], preferred_element_type=F32)
            dbuf[rows, s * 128 : (s + 1) * 128] = both[:, 0:128] * scale
            vbuf[rows, s * 128 : (s + 1) * 128] = gelu(both[:, 128:256] * scale)
        for s in range(2):
            slot = pair * 2 + s
            v = vbuf[pl.ds(slot * R, R), :]
            total = jnp.sum(v, axis=1, keepdims=True)
            squares = jnp.sum(v * v, axis=1, keepdims=True)
            tile = jnp.where(lane == 0, total, jnp.where(lane == 1, squares, 0.0))
            stat[0, block_of[slot]] = jnp.transpose(tile)[0:8, :]

    def mixing(pair):
        for s in range(2):
            slot = pair * 2 + s
            rows = pl.ds(slot * R, R)
            block = block_of[slot]
            sums = stat[0, block] + stat[1, block] + stat[2, block] + stat[3, block]
            tile = jnp.transpose(jnp.concatenate([sums] * 16, axis=0))
            mean = tile[:, 0:1] / BRANCH
            var = tile[:, 1:2] / BRANCH - mean * mean
            inv = lax.rsqrt(var + EPS)
            for k in range(2):
                lanes = slice(k * 128, (k + 1) * 128)
                v = vbuf[rows, lanes]
                g = ((v - mean) * inv * small[k, 0:1, :] + small[k, 1:2, :]).astype(BF16)
                low = jnp.dot(swb[k, 0], g, preferred_element_type=F32)
                high = jnp.dot(swb[k, 1], g, preferred_element_type=F32)
                mixed = jnp.where(lane < 64, low, high) + bias[k]
                gbuf[rows, lanes] = (gelu(dbuf[rows, lanes]) * mixed).astype(BF16)
        rows = pl.ds(pair * 256, 256)

        @pl.loop(0, 8)
        def _(j):
            first = pl.ds(pl.multiple_of(j * 256, 128), 128)
            second = pl.ds(pl.multiple_of(j * 256 + 128, 128), 128)
            weights = jnp.concatenate(
                [
                    jnp.concatenate([mixw[k, first, 256:384], mixw[k, second, 256:384]], axis=1)
                    for k in range(2)
                ],
                axis=0,
            )
            product = jnp.dot(gbuf[rows, :], weights, preferred_element_type=F32)
            part1[rows, pl.ds(pl.multiple_of(j * 256, 256), 256)] = product.astype(BF16)

    def feed(pair):
        rows = pl.ds(pair * 256, 256)
        row_scales(x2buf, pair)

        @pl.loop(0, 8)
        def _(j):
            cols = pl.ds(pl.multiple_of(lax.rem(j, 4) * 256, 256), 256)
            upper = jnp.dot(x2buf[rows, :], we[lax.div(j, 4), :, cols], preferred_element_type=F32)
            scale = rbuf[rows, :]
            upper = upper * jnp.concatenate([scale, scale], axis=1)
            hidden = jnp.square(jnp.maximum(upper, 0.0)).astype(BF16)
            hbuf[:, pl.ds(pl.multiple_of(j * 256, 256), 256)] = hidden

        @pl.loop(0, 8)
        def _(j):
            weights = jnp.concatenate([wr[2 * j], wr[2 * j + 1]], axis=1)
            product = jnp.dot(hbuf[...], weights, preferred_element_type=F32)
            part2[rows, pl.ds(pl.multiple_of(j * 256, 256), 256)] = product.astype(BF16)

    gather_near(xbuf, 0)
    pltpu.make_async_remote_copy(
        src_ref=mixw.at[other, pl.ds(0, 1024)],
        dst_ref=mixw.at[other, pl.ds(0, 1024)],
        send_sem=w_send_d2d.at[0],
        recv_sem=w_recv_d2d.at[0],
        device_id=sib,
        device_id_type=MESH,
    ).wait_recv()
    pltpu.make_async_remote_copy(
        src_ref=mixw.at[other, pl.ds(1024, 1024)],
        dst_ref=mixw.at[other, pl.ds(1024, 1024)],
        send_sem=w_send_d2d.at[1],
        recv_sem=w_recv_d2d.at[1],
        device_id=sib,
        device_id_type=MESH,
    ).wait_recv()
    project(0)
    gather_far(xbuf, 0)
    project(1)
    stat_copies = [
        rcopy(stat.at[0], stat.at[k + 1], st_send.at[k], st_recv.at[k], to)
        for k, to in enumerate((ynext, yprev, yfar))
    ]
    for copy in stat_copies:
        copy.start()
    rcopy(small.at[other], small.at[other], sm_send.at[0], sm_recv.at[0], sib).wait_recv()
    rcopy(swb.at[other], swb.at[other], sm_send.at[1], sm_recv.at[1], sib).wait_recv()
    for k in range(2):
        rows = jnp.concatenate(
            [jnp.broadcast_to(small[k, 2 + g : 3 + g, :], (64, 128)) for g in range(2)], axis=0
        )
        bias[k] = jnp.transpose(rows)
    for copy in stat_copies:
        copy.wait_recv()
    mixing(0)
    for way in range(2):
        scatter_own(part1, 0, way).start()
    mixing(1)
    for k in range(2):
        for way in range(2):
            scatter_far(part1, 0, way, k).start()
    expand.wave1()
    reduce.wave1()
    scatter_join(part1, 0)

    def middle_done(row, value):
        x2buf[pl.ds(SO * R + row, CHUNK), :] = value
        for way in range(2):
            gather_copy(x2buf, 1, way, ORDER.index(row)).start()

    scatter_finish(part1, 0, xbuf, middle_done)
    expand.wave2()
    reduce.wave2()
    gather_pass_on(x2buf, 1)
    expand.wave3()
    reduce.wave3()
    expand.wave4()
    reduce.wave4()

    gather_near(x2buf, 1)
    rcopy(we.at[other], we.at[other], w_send_d2d.at[2], w_recv_d2d.at[2], sib).wait_recv()
    half = wr.at[:, pl.ds(pl.multiple_of(other * HW, HW), HW)]
    rcopy(half, half, w_send_d2d.at[3], w_recv_d2d.at[3], sib).wait_recv()
    feed(0)
    for way in range(2):
        scatter_own(part2, 1, way).start()
    gather_far(x2buf, 1)
    feed(1)
    for k in range(2):
        for way in range(2):
            scatter_far(part2, 1, way, k).start()
    scatter_join(part2, 1)

    def result_done(row, value):
        out[pl.ds(row, CHUNK), :] = value

    scatter_finish(part2, 1, x2buf, result_done)

    for phase, buf, part in ((0, xbuf, part1), (1, x2buf, part2)):
        for way in range(2):
            for k in range(6):
                gather_copy(buf, phase, way, k).wait_send()
            scatter_own(part, phase, way).wait_send()
            for k in range(2):
                scatter_far(part, phase, way, k).wait_send()
                scatter_joined(phase, way, k).wait_send()
    for copy in (*stat_copies, small_copy, spatial_copy):
        copy.wait_send()
    sent = (
        (mixw.at[c, pl.ds(0, 960)], mixw.at[c, pl.ds(0, 1024)]),
        (mixw.at[c, pl.ds(0, 960)], mixw.at[c, pl.ds(0, 1024)]),
        (we.at[c, pl.ds(0, 1920)], we.at[c]),
        (wr.at[pl.ds(0, 15), pl.ds(0, HW)], wr.at[:, pl.ds(0, HW)]),
    )
    for index, (torus, across) in enumerate(sent):
        rcopy(torus, torus, w_send.at[index], w_recv_d2d.at[index], sib).wait_send()
        rcopy(across, across, w_send_d2d.at[index], w_recv_d2d.at[index], sib).wait_send()


def layer(*args):
    (
        tokens,
        mixer_gain,
        direct_weight,
        direct_scale,
        value_weight,
        value_scale,
        value_gain,
        value_shift,
        spatial_weight,
        spatial_bias,
        merge_weight,
        merge_scale,
        channel_gain,
        expand_weight,
        expand_scale,
        reduce_weight,
        reduce_scale,
    ) = args
    operands = (
        tokens,
        mixer_gain.reshape(16, 128),
        direct_weight,
        direct_scale.reshape(1, CW),
        value_weight,
        value_scale.reshape(1, CW),
        value_gain.reshape(1, CW),
        value_shift.reshape(1, CW),
        spatial_weight,
        spatial_bias,
        merge_weight,
        merge_scale.reshape(1, 128),
        channel_gain.reshape(16, 128),
        expand_weight,
        expand_scale.reshape(1, HW),
        reduce_weight,
        reduce_scale.reshape(1, 128),
    )
    vmem = pl.BlockSpec(memory_space=pltpu.VMEM)
    dma = pltpu.SemaphoreType.DMA
    return pl.pallas_call(
        kernel,
        out_shape=jax.ShapeDtypeStruct((R, D), BF16),
        in_specs=[pl.BlockSpec(memory_space=pl.ANY)] + [vmem] * 16,
        out_specs=vmem,
        scratch_shapes=[
            pltpu.VMEM((2, D, 384), BF16),
            pltpu.VMEM((2, D, HW), BF16),
            pltpu.VMEM((16, 2 * HW, 128), BF16),
            pltpu.VMEM((4 * R, D), BF16),
            pltpu.VMEM((4 * R, D), BF16),
            pltpu.VMEM((4 * R, D), BF16),
            pltpu.VMEM((4 * R, D), BF16),
            pltpu.VMEM((2, 2, 64, D), BF16),
            pltpu.VMEM((2, 2, R, D), BF16),
            pltpu.VMEM((2, 2, 64, D), BF16),
            pltpu.VMEM((2 * R, D), BF16),
            pltpu.VMEM((4 * R, 256), F32),
            pltpu.VMEM((4 * R, 256), F32),
            pltpu.VMEM((4 * R, 256), BF16),
            pltpu.VMEM((4 * R, 128), F32),
            pltpu.VMEM((4, 4, 8, 128), F32),
            pltpu.VMEM((2, 8, 128), F32),
            pltpu.VMEM((2, 2, 128, 128), BF16),
            pltpu.VMEM((2, 128, 128), F32),
            dma,
            dma((2, 2, 6)),
            dma((2, 2, 6)),
            dma((2, 2, 5)),
            dma((2, 2, 5)),
            dma((3,)),
            dma((3,)),
            dma((2,)),
            dma((2,)),
            dma((4,)),
            dma((4,)),
            dma((4, 4)),
            dma((4, 4, 4)),
            dma((4,)),
        ],
        compiler_params=pltpu.CompilerParams(
            collective_id=0, has_side_effects=True, vmem_limit_bytes=60 * 1024 * 1024
        ),
        name="layer",
    )(*operands)


def solution(mesh):
    finer = Mesh(mesh.devices.reshape(2, 4, 4, 4, 2), AXES)
    in_specs = (
        P(AXES, None),
        P(),
        P(FS, TP),
        P(TP),
        P(FS, TP),
        P(TP),
        P(TP),
        P(TP),
        P(TP, None, None),
        P(TP, None),
        P(TP, FS),
        P(FS),
        P(),
        P(FS, TP),
        P(TP),
        P(TP, FS),
        P(FS),
    )
    return jax.shard_map(layer, mesh=finer, in_specs=in_specs, out_specs=P(AXES, None), check_vma=False)
```

time: 339 us -> 111 us (0.33)
  blocking collectives: 225 us -> 0 us
  Pallas kernels: 0 us -> 109 us
  matrix products: 27 us -> 0 us
  starting transfers between devices: 24.4 us -> 0 us
  other arithmetic: 17.1 us -> 0 us
  local copies, waits for them, and re-layouts: 16 us -> 1.88 us
  waiting for transfers between devices: 14.1 us -> 0 us
  between operations: 13.4 us -> 0.01 us
    all_to_all x6 -> x0, blocking collectives: 118 us -> none  [the longest x2 59.3 us: sum_in_two_steps(): lax.all_to_all(own.astype(jnp.bfloat16), far, 0, 0, tiled=True)]
    pallas_call x0 -> x1, Pallas kernels: none -> 109 us  [layer(): pl.pallas_call(kernel, out_shape=jax.ShapeDtypeStruct((R, D), BF16), in_s...]
    all_gather x3 -> x0, blocking collectives: 108 us -> none  [the longest x1 40.5 us: body(): lax.all_gather(merge_half, 'fs', axis=1, tiled=True)]
    dot_general x4 -> x0, matrix products: 27 us -> none  [the longest x1 14.4 us: body(): jnp.dot(rows, full_reduce, preferred_element_type=jnp.float32)]
    all_to_all x3 -> x0, starting transfers between devices: 24.3 us -> none  [copy_for_each(): return lax.all_to_all(copies, axis, split_axis=0, concat_axis=0, tiled=True)]
    all_gather x3 -> x0, waiting for transfers between devices: 14 us -> none  [the longest x1 8.52 us: body(): lax.all_gather(expand_half, 'fs', axis=0, tiled=True)]
    reduce_sum x7 -> x0, other arithmetic: 9.47 us -> none  [the longest x2 7.13 us: sent_and_summed(): return arrived.astype(jnp.float32).sum(axis=0)]
    convert_element_type x11 -> x0, other arithmetic: 6.95 us -> none  [the longest x1 1.77 us: body(): reduce_half = reduce_weight.astype(jnp.bfloat16)]
  transfers between devices with their start and end apart: 6 -> 0, of which waited for: 2 -> 0; matrix products, arithmetic and copies ran while one was open for 11% -> 0% of each run, Pallas kernels for 0% -> 0%
where the time goes in v1:
time: 111 us
  Pallas kernels  109 us (98%)
  local copies, waits for them, and re-layouts  1.88 us (2%)
    pallas_call x1, Pallas kernels, layer(): pl.pallas_call(kernel, out_shape=jax.ShapeDtypeStruct((R, D), BF16), in_s...  109 us

profile of v1, /device:TPU:1, one launch (start us, length us, event | category | flops | bytes accessed | tf_op | source)
XLA Modules:
  0.0 111.2 jit_solution(6863148947125497457)
XLA Ops:
  0.0 109.3 %layer.1 = bf16[128,2048]{1,0:T(8,128)(2,1)} custom-call(bf16[128,2048]{1,0:T(8,128)(2,1)} %tokens.1, f32[16,128]{1,0:T(8,128)} %bitcast.9, f32[128,128]{1,0:T(8,128)} %direct_weight.1, f32[1,128]{1,0:T(1,128)} %bitcast.12, f32[128,128]{1,0:T(8,128)} %value_weight.1, f32[1,128]{1,0:T(1,128)} %bitcast.13, f32[1,128]{1,0:T(1,128)} %bitcast.14, ...), custom_call_target="tpu_custom_call" | custom-call | tf_op jit(solution)/shard_map/layer/pallas_call | solution.py:591
  109.3 1.9 %copy.19 = bf16[128,2048]{1,0:T(8,128)(2,1)} copy(bf16[128,2048]{1,0:T(8,128)(2,1)} %layer.1) | data formatting | bytes 1048576

commit v2 on v1

v2 whole, which is shorter than its diff:
```python
import functools

import jax
import jax.numpy as jnp
from jax import lax
from jax.experimental import pallas as pl
from jax.experimental.pallas import tpu as pltpu
from jax.sharding import Mesh
from jax.sharding import PartitionSpec as P

AXES = ("zh", "zl", "x", "y", "c")
FS = ("zl", "x")
TP = ("y", "c")
EPS = 1e-6
MESH = pl.DeviceIdType.MESH
F32 = jnp.float32
BF16 = jnp.bfloat16

D = 2048
R = 128
CW = 128
HW = 1024
BRANCH = 1024
SN, SP, SF, SO = 0, 1, 2, 3
CHUNK = 32


def gelu(u):
    return jax.nn.gelu(u, approximate=True)


class Gather:
    def __init__(self, view, a, b, pa, pb, sib, send, send_d2d, recv_a, recv_b, recv_d2d):
        self.view, self.a, self.b, self.sib = view, a, b, sib
        self.pa, self.pb = pa, pb
        self.send, self.send_d2d = send, send_d2d
        self.recv_a, self.recv_b, self.recv_d2d = recv_a, recv_b, recv_d2d

    def item(self, da, db, half=None):
        return self.view(lax.rem(self.pa + 4 - da, 4), lax.rem(self.pb + 4 - db, 4), half)

    def copy(self, ref, sem, to):
        return pltpu.make_async_remote_copy(
            src_ref=ref, dst_ref=ref, send_sem=self.send, recv_sem=sem, device_id=to, device_id_type=MESH
        )

    def along_b(self, da):
        ref = self.item(da, 0)
        self.copy(ref, self.recv_b.at[da, 0], self.b[0]).start()
        self.copy(ref, self.recv_b.at[da, 1], self.b[1]).start()

    def across(self, da, db):
        ref = self.item(da, db)
        pltpu.make_async_remote_copy(
            src_ref=ref,
            dst_ref=ref,
            send_sem=self.send_d2d,
            recv_sem=self.recv_d2d,
            device_id=self.sib,
            device_id_type=MESH,
        ).start()

    def landed(self, ref, sem):
        self.copy(ref, sem, self.sib).wait_recv()

    def near_a(self, k):
        da = (1, 3)[k]
        self.landed(self.item(da, 0), self.recv_a.at[k])
        self.copy(self.item(da, 0, k), self.recv_a.at[2 + k], self.a[k]).start()
        self.along_b(da)
        self.across(da, 0)

    def near_b(self, da):
        for k in range(2):
            db = (1, 3)[k]
            self.landed(self.item(da, db), self.recv_b.at[da, k])
            self.copy(self.item(da, db, k), self.recv_b.at[da, 2 + k], self.b[k]).start()
            self.across(da, db)

    def far_b(self, da):
        for k in range(2):
            self.landed(self.item(da, 2, k), self.recv_b.at[da, 2 + k])
        self.across(da, 2)

    def wave0(self):
        ref = self.item(0, 0)
        for k in range(2):
            self.copy(ref, self.recv_a.at[k], self.a[k]).start()
        self.along_b(0)
        self.across(0, 0)

    def wave1(self):
        for k in range(2):
            self.near_a(k)
        self.near_b(0)

    def wave2(self):
        for k in range(2):
            self.landed(self.item(2, 0, k), self.recv_a.at[2 + k])
        self.along_b(2)
        self.across(2, 0)
        self.near_b(1)
        self.near_b(3)
        self.far_b(0)

    def wave3(self):
        self.near_b(2)
        self.far_b(1)
        self.far_b(3)

    def wave4(self):
        self.far_b(2)


def kernel(
    tokens,
    mixer_gain_hbm,
    direct_weight_hbm,
    direct_scale_hbm,
    value_weight_hbm,
    value_scale_hbm,
    value_gain_hbm,
    value_shift_hbm,
    spatial_weight_hbm,
    spatial_bias_hbm,
    merge_weight_hbm,
    merge_scale_hbm,
    channel_gain_hbm,
    expand_weight_hbm,
    expand_scale_hbm,
    reduce_weight_hbm,
    reduce_scale_hbm,
    out,
    mixer_gain,
    direct_weight,
    direct_scale,
    value_weight,
    value_scale,
    value_gain,
    value_shift,
    spatial_weight,
    spatial_bias,
    merge_weight,
    merge_scale,
    channel_gain,
    expand_weight,
    expand_scale,
    reduce_weight,
    reduce_scale,
    valw,
    dmw,
    we,
    wr,
    xbuf,
    x2buf,
    part1,
    part2,
    rel,
    near,
    mrg,
    hbuf,
    dbuf,
    vbuf,
    gbuf,
    rbuf,
    stat,
    small,
    swb,
    bias,
    in_sem,
    ag_send,
    ag_recv,
    rs_send,
    rs_recv,
    st_send,
    st_recv,
    sm_send,
    sm_recv,
    w_send,
    w_send_d2d,
    w_recv_a,
    w_recv_b,
    w_recv_d2d,
):
    zh, zl, x, y, c = (lax.axis_index(name) for name in AXES)
    z = zh * 4 + zl
    fs = zl * 4 + x
    other = 1 - c
    scope = jax.named_scope

    def at_z(w):
        w = lax.rem(w, 8)
        return {"zh": lax.div(w, 4), "zl": lax.rem(w, 4)}

    xs = ({"x": lax.rem(x + 1, 4)}, {"x": lax.rem(x + 3, 4)})
    zs = (at_z(z + 1), at_z(z + 7))
    ynext, yprev, yfar = ({"y": lax.rem(y + k, 4)} for k in (1, 3, 2))
    sib = {"c": other}

    barrier = pltpu.get_barrier_semaphore()
    for to in (*xs, *zs, ynext, yprev, yfar, sib):
        pl.semaphore_signal(barrier, inc=1, device_id=to, device_id_type=MESH)

    inputs = [
        pltpu.make_async_copy(src, dst, in_sem.at[k])
        for k, (src, dst) in enumerate(
            (
                (tokens, xbuf.at[pl.ds(SO * R, R)]),
                (mixer_gain_hbm, mixer_gain),
                (direct_weight_hbm, direct_weight),
                (direct_scale_hbm, direct_scale),
                (value_weight_hbm, value_weight),
                (value_scale_hbm, value_scale),
                (merge_weight_hbm, merge_weight),
                (merge_scale_hbm, merge_scale),
                (channel_gain_hbm, channel_gain),
                (expand_weight_hbm, expand_weight),
                (expand_scale_hbm, expand_scale),
                (reduce_weight_hbm, reduce_weight),
                (reduce_scale_hbm, reduce_scale),
                (value_gain_hbm, value_gain),
                (value_shift_hbm, value_shift),
                (spatial_bias_hbm, spatial_bias),
                (spatial_weight_hbm, spatial_weight),
            )
        )
    ]
    for copy in inputs:
        copy.start()

    def rcopy(src, dst, ssem, rsem, to):
        return pltpu.make_async_remote_copy(
            src_ref=src, dst_ref=dst, send_sem=ssem, recv_sem=rsem, device_id=to, device_id_type=MESH
        )

    def gather_copy(buf, phase, way, k):
        if k < 4:
            src = buf.at[pl.ds(SO * R + CHUNK * k, CHUNK)]
            dst = buf.at[pl.ds((SP, SN)[way] * R + CHUNK * k, CHUNK)]
        else:
            row = 64 * way + CHUNK * (k - 4)
            src = buf.at[pl.ds((SP, SN)[way] * R + row, CHUNK)]
            dst = buf.at[pl.ds(SF * R + row, CHUNK)]
        return rcopy(
            src, dst, ag_send.at[phase, way, k], ag_recv.at[phase, way, k], (ynext, yprev)[way]
        )

    def gather_pass_on(buf, phase, k):
        for way in range(2):
            gather_copy(buf, phase, way, 2 * way + k).wait_recv()
            gather_copy(buf, phase, way, 4 + k).start()

    def gather_near(buf, phase):
        for way in range(2):
            for k in range(2):
                gather_copy(buf, phase, way, 2 * (1 - way) + k).wait_recv()

    def gather_far(buf, phase):
        for way in range(2):
            for k in range(2):
                gather_copy(buf, phase, way, 4 + k).wait_recv()

    def scatter_own(part, phase, way):
        rows = pl.ds(64 * (1 - way), 64)
        src = part.at[pl.ds((SN, SP)[way] * R + 64 * (1 - way), 64)]
        return rcopy(
            src,
            near.at[phase, way, rows],
            rs_send.at[phase, way, 0],
            rs_recv.at[phase, way, 0],
            (ynext, yprev)[way],
        )

    def scatter_far(part, phase, way, k):
        row = CHUNK * k
        return rcopy(
            part.at[pl.ds(SF * R + 64 * way + row, CHUNK)],
            rel.at[phase, way, pl.ds(row, CHUNK)],
            rs_send.at[phase, way, 1 + k],
            rs_recv.at[phase, way, 1 + k],
            (ynext, yprev)[way],
        )

    def scatter_joined(phase, way, k):
        row = CHUNK * k
        return rcopy(
            mrg.at[phase, way, pl.ds(row, CHUNK)],
            near.at[phase, way, pl.ds(64 * way + row, CHUNK)],
            rs_send.at[phase, way, 3 + k],
            rs_recv.at[phase, way, 3 + k],
            (ynext, yprev)[way],
        )

    def scatter_join(part, phase, k):
        for way in range(2):
            row = CHUNK * k
            scatter_far(part, phase, way, k).wait_recv()
            mine = part[pl.ds((SN, SP)[way] * R + 64 * way + row, CHUNK), :].astype(F32)
            came = rel[phase, way, pl.ds(row, CHUNK), :].astype(F32)
            mrg[phase, way, pl.ds(row, CHUNK), :] = (mine + came).astype(BF16)
            scatter_joined(phase, way, k).start()

    def scatter_finish(part, phase, base, done, k):
        if k == 0:
            for way in range(2):
                scatter_own(part, phase, way).wait_recv()
        for way in range(2):
            scatter_joined(phase, way, k).wait_recv()
            row = 64 * way + CHUNK * k
            total = part[pl.ds(SO * R + row, CHUNK), :].astype(F32)
            total = total + near[phase, 0, pl.ds(row, CHUNK), :].astype(F32)
            total = total + near[phase, 1, pl.ds(row, CHUNK), :].astype(F32)
            mine = base[pl.ds(SO * R + row, CHUNK), :].astype(F32)
            done(row, (mine + total).astype(BF16))

    def view_rows(ref, low):
        def view(pz, px, half):
            row = (pz * 4 + px) * 128 + low
            if half is None:
                return ref.at[c, pl.ds(pl.multiple_of(row, 64), 64)]
            return ref.at[c, pl.ds(pl.multiple_of(row + 32 * half, 32), 32)]

        return view

    def view_reduce(low):
        def view(pz, px, half):
            row = c * HW + low
            if half is None:
                return wr.at[pz * 4 + px, pl.ds(pl.multiple_of(row, 512), 512)]
            return wr.at[pz * 4 + px, pl.ds(pl.multiple_of(row + 256 * half, 256), 256)]

        return view

    def weight(index, view, x_first):
        if x_first:
            a, b, pa, pb, turned = xs, zs, x, zl, lambda p, q, h: view(q, p, h)
        else:
            a, b, pa, pb, turned = zs, xs, zl, x, view
        return Gather(
            turned,
            a,
            b,
            pa,
            pb,
            sib,
            w_send.at[index],
            w_send_d2d.at[index],
            w_recv_a.at[index],
            w_recv_b.at[index],
            w_recv_d2d.at[index],
        )

    class Pair:
        def __init__(self, index, low, high):
            self.halves = (weight(index, low, True), weight(index + 1, high, False))

        def wave(self, k):
            for half in self.halves:
                getattr(half, f"wave{k}")()

    value_blocks = Pair(0, view_rows(valw, 0), view_rows(valw, 64))
    dm_blocks = Pair(2, view_rows(dmw, 0), view_rows(dmw, 64))
    expand_blocks = Pair(4, view_rows(we, 0), view_rows(we, 64))
    reduce_blocks = Pair(6, view_reduce(0), view_reduce(512))

    def column(row):
        return jnp.transpose(jnp.broadcast_to(row, (128, 128)))

    with scope("wait_tokens"):
        inputs[0].wait()
    with scope("wait_barrier"):
        pl.semaphore_wait(barrier, 8)
    for k in range(4):
        for way in range(2):
            gather_copy(xbuf, 0, way, (k + 2 * way) % 4).start()
    with scope("wait_mix"):
        for copy in inputs[1:8]:
            copy.wait()

    fs_row = pl.ds(pl.multiple_of(fs * 128, 128), 128)
    gain = column(mixer_gain[pl.ds(fs, 1), :])
    valw[c, fs_row, :] = (value_weight[...] * gain * value_scale[...]).astype(BF16)
    dmw[c, fs_row, 0:128] = (direct_weight[...] * gain * direct_scale[...]).astype(BF16)
    dmw[c, fs_row, 128:256] = (merge_weight[...] * merge_scale[...]).astype(BF16)
    value_blocks.wave(0)
    dm_blocks.wave(0)
    for copy in inputs[8:]:
        copy.wait()
    gain = column(channel_gain[pl.ds(fs, 1), :])
    for k in range(8):
        lanes = slice(k * 128, (k + 1) * 128)
        we[c, fs_row, lanes] = (expand_weight[:, lanes] * gain * expand_scale[:, lanes]).astype(BF16)
    for k in range(8):
        rows = pl.ds(pl.multiple_of(c * HW + k * 128, 128), 128)
        wr[fs, rows, :] = (reduce_weight[k * 128 : (k + 1) * 128, :] * reduce_scale[...]).astype(BF16)
    small[c, 0:1, :] = value_gain[...]
    small[c, 1:2, :] = value_shift[...]
    small[c, 2:4, :] = spatial_bias[...]
    small[c, 4:8, :] = jnp.zeros((4, 128), F32)
    swb[c] = spatial_weight[...]
    small_copy = rcopy(small.at[c], small.at[c], sm_send.at[0], sm_recv.at[0], sib)
    spatial_copy = rcopy(spatial_weight, swb.at[c], sm_send.at[1], sm_recv.at[1], sib)
    small_copy.start()
    spatial_copy.start()

    with scope("v_w1"):
        value_blocks.wave(1)
    with scope("dm_w1"):
        dm_blocks.wave(1)
    expand_blocks.halves[0].wave0()
    with scope("v_w2"):
        value_blocks.wave(2)
    with scope("pass1_0"):
        gather_pass_on(xbuf, 0, 0)
    with scope("dm_w2"):
        dm_blocks.wave(2)
    with scope("v_w3"):
        value_blocks.wave(3)
    expand_blocks.halves[1].wave0()
    with scope("pass1_1"):
        gather_pass_on(xbuf, 0, 1)
    with scope("dm_w3"):
        dm_blocks.wave(3)
    with scope("v_w4"):
        value_blocks.wave(4)
    with scope("e_w1"):
        expand_blocks.wave(1)

    def row_scales(buf, start, count):
        @pl.loop(0, count // 32)
        def _(i):
            rows = pl.ds(pl.multiple_of(start + i * 32, 32), 32)
            floats = buf[rows, :].astype(F32)
            power = jnp.mean(floats * floats, axis=-1, keepdims=True)
            rbuf[rows, :] = jnp.broadcast_to(lax.rsqrt(power + EPS), (32, 128))

    lane = lax.broadcasted_iota(jnp.int32, (128, 128), 1)
    block_of = {SP: lax.rem(y + 3, 4), SN: lax.rem(y + 1, 4), SF: lax.rem(y + 2, 4), SO: y}

    def project(slots):
        start, count = slots[0] * R, len(slots) * R
        row_scales(xbuf, start, count)
        rows = pl.ds(start, count)
        weights = jnp.concatenate([valw[0], valw[1]], axis=1)
        value = jnp.dot(xbuf[rows, :], weights, preferred_element_type=F32)
        scale = rbuf[rows, :]
        vbuf[rows, :] = gelu(value * jnp.concatenate([scale, scale], axis=1))
        for slot in slots:
            v = vbuf[pl.ds(slot * R, R), :]
            total = jnp.sum(v, axis=1, keepdims=True)
            squares = jnp.sum(v * v, axis=1, keepdims=True)
            tile = jnp.where(lane == 0, total, jnp.where(lane == 1, squares, 0.0))
            stat[0, block_of[slot]] = jnp.transpose(tile)[0:8, :]

    def project_direct():
        weights = jnp.concatenate([dmw[0, :, 0:128], dmw[1, :, 0:128]], axis=1)

        @pl.loop(0, 2)
        def _(i):
            rows = pl.ds(pl.multiple_of(i * 256, 256), 256)
            direct = jnp.dot(xbuf[rows, :], weights, preferred_element_type=F32)
            scale = rbuf[rows, :]
            dbuf[rows, :] = gelu(direct * jnp.concatenate([scale, scale], axis=1))

    def mixing(slots):
        for slot in slots:
            rows = pl.ds(slot * R, R)
            block = block_of[slot]
            sums = stat[0, block] + stat[1, block] + stat[2, block] + stat[3, block]
            tile = jnp.transpose(jnp.concatenate([sums] * 16, axis=0))
            mean = tile[:, 0:1] / BRANCH
            var = tile[:, 1:2] / BRANCH - mean * mean
            inv = lax.rsqrt(var + EPS)
            for k in range(2):
                lanes = slice(k * 128, (k + 1) * 128)
                v = vbuf[rows, lanes]
                g = ((v - mean) * inv * small[k, 0:1, :] + small[k, 1:2, :]).astype(BF16)
                low = jnp.dot(swb[k, 0], g, preferred_element_type=F32)
                high = jnp.dot(swb[k, 1], g, preferred_element_type=F32)
                mixed = jnp.where(lane < 64, low, high) + bias[k]
                gbuf[rows, lanes] = (dbuf[rows, lanes] * mixed).astype(BF16)
        rows = pl.ds(slots[0] * R, len(slots) * R)

        @pl.loop(0, 2)
        def _(j):
            weights = jnp.concatenate(
                [
                    jnp.concatenate(
                        [
                            dmw[k, pl.ds(pl.multiple_of(j * 1024 + i * 128, 128), 128), 128:256]
                            for i in range(8)
                        ],
                        axis=1,
                    )
                    for k in range(2)
                ],
                axis=0,
            )
            product = jnp.dot(gbuf[rows, :], weights, preferred_element_type=F32)
            part1[rows, pl.ds(pl.multiple_of(j * 1024, 1024), 1024)] = product.astype(BF16)

    def gathered_rows(ref, pieces):
        loaded = [ref[pl.ds(start, count), :] for start, count in pieces]
        return loaded[0] if len(loaded) == 1 else jnp.concatenate(loaded, axis=0)

    def store_rows(ref, pieces, cols, values):
        at = 0
        for start, count in pieces:
            ref[pl.ds(start, count), cols] = values[at : at + count, :]
            at += count

    def feed_up(pieces):
        for start, count in pieces:
            row_scales(x2buf, start, count)

        @pl.loop(0, 2)
        def _(j):
            upper = jnp.dot(gathered_rows(x2buf, pieces), we[j], preferred_element_type=F32)
            upper = upper * jnp.concatenate([gathered_rows(rbuf, pieces)] * 8, axis=1)
            hidden = jnp.square(jnp.maximum(upper, 0.0)).astype(BF16)
            store_rows(hbuf, pieces, pl.ds(pl.multiple_of(j * HW, HW), HW), hidden)

    def feed_down(pieces):
        @pl.loop(0, 2)
        def _(j):
            weights = jnp.concatenate([wr[8 * j + i] for i in range(8)], axis=1)
            product = jnp.dot(gathered_rows(hbuf, pieces), weights, preferred_element_type=F32)
            store_rows(part2, pieces, pl.ds(pl.multiple_of(j * 1024, 1024), 1024), product.astype(BF16))

    def shared(ref, index):
        rcopy(ref, ref, w_send_d2d.at[index], w_recv_d2d.at[index], sib).wait_recv()

    with scope("v_d2d"):
        shared(valw.at[other, pl.ds(0, 1024)], 0)
        shared(valw.at[other, pl.ds(1024, 1024)], 1)
    with scope("project_own"):
        project((SO,))
    with scope("dm_w4"):
        dm_blocks.wave(4)
    with scope("near1"):
        gather_near(xbuf, 0)
    with scope("project_near"):
        project((SN, SP))
    with scope("far1"):
        gather_far(xbuf, 0)
    with scope("project_far"):
        project((SF,))
    stat_copies = [
        rcopy(stat.at[0], stat.at[k + 1], st_send.at[k], st_recv.at[k], to)
        for k, to in enumerate((ynext, yprev, yfar))
    ]
    for copy in stat_copies:
        copy.start()
    reduce_blocks.wave(0)
    with scope("dm_d2d"):
        shared(dmw.at[other, pl.ds(0, 1024)], 2)
        shared(dmw.at[other, pl.ds(1024, 1024)], 3)
    with scope("direct"):
        project_direct()
        rcopy(small.at[other], small.at[other], sm_send.at[0], sm_recv.at[0], sib).wait_recv()
        rcopy(swb.at[other], swb.at[other], sm_send.at[1], sm_recv.at[1], sib).wait_recv()
        for k in range(2):
            rows = jnp.concatenate(
                [jnp.broadcast_to(small[k, 2 + g : 3 + g, :], (64, 128)) for g in range(2)], axis=0
            )
            bias[k] = jnp.transpose(rows)
    with scope("wait_stats"):
        for copy in stat_copies:
            copy.wait_recv()
    with scope("mixing_near"):
        mixing((SN, SP))
    for way in range(2):
        scatter_own(part1, 0, way).start()
    with scope("mixing_far"):
        mixing((SF,))
    for k in range(2):
        for way in range(2):
            scatter_far(part1, 0, way, k).start()
    with scope("mixing_own"):
        mixing((SO,))
    with scope("e_w2"):
        expand_blocks.wave(2)
    with scope("r_w1"):
        reduce_blocks.wave(1)
    with scope("join1_0"):
        scatter_join(part1, 0, 0)
    with scope("join1_1"):
        scatter_join(part1, 0, 1)
    with scope("e_w3"):
        expand_blocks.wave(3)

    def middle_done(row, value):
        x2buf[pl.ds(SO * R + row, CHUNK), :] = value

    with scope("finish1_0"):
        scatter_finish(part1, 0, xbuf, middle_done, 0)
    for way in range(2):
        gather_copy(x2buf, 1, way, 2 * way).start()
    with scope("finish1_1"):
        scatter_finish(part1, 0, xbuf, middle_done, 1)
    for way in range(2):
        gather_copy(x2buf, 1, way, 2 * way + 1).start()
    with scope("r_w2"):
        reduce_blocks.wave(2)
    with scope("pass2_0"):
        gather_pass_on(x2buf, 1, 0)
    with scope("e_w4"):
        expand_blocks.wave(4)
    with scope("pass2_1"):
        gather_pass_on(x2buf, 1, 1)
    for k in range(2):
        for way in range(2):
            gather_copy(x2buf, 1, way, 2 * (1 - way) + k).start()

    outer, inner = ((64, 128),), ((0, 64), (192, 64))
    far, own = ((SF * R, R),), ((SO * R, R),)
    with scope("e_d2d"):
        shared(we.at[other, pl.ds(0, 1024)], 4)
        shared(we.at[other, pl.ds(1024, 1024)], 5)
    with scope("up_outer"):
        feed_up(outer)
    with scope("r_w3"):
        reduce_blocks.wave(3)
    with scope("up_own"):
        feed_up(own)
    with scope("r_w4"):
        reduce_blocks.wave(4)
    with scope("r_d2d"):
        shared(wr.at[pl.ds(0, 8), pl.ds(pl.multiple_of(other * HW, HW), HW)], 6)
        shared(wr.at[pl.ds(8, 8), pl.ds(pl.multiple_of(other * HW, HW), HW)], 7)
    with scope("down_outer"):
        feed_down(outer)
    for way in range(2):
        scatter_own(part2, 1, way).start()
    with scope("far2"):
        gather_far(x2buf, 1)
    with scope("feed_far"):
        feed_up(far)
        feed_down(far)
    for k in range(2):
        for way in range(2):
            scatter_far(part2, 1, way, k).start()
    with scope("near2"):
        gather_near(x2buf, 1)
    with scope("feed_inner"):
        feed_up(inner)
        feed_down(inner)
    with scope("down_own"):
        feed_down(own)
    with scope("join2_0"):
        scatter_join(part2, 1, 0)
    with scope("join2_1"):
        scatter_join(part2, 1, 1)

    def result_done(row, value):
        out[pl.ds(row, CHUNK), :] = value

    with scope("finish2_0"):
        scatter_finish(part2, 1, x2buf, result_done, 0)
    with scope("finish2_1"):
        scatter_finish(part2, 1, x2buf, result_done, 1)

    with scope("drain"):
        for phase, buf, part in ((0, xbuf, part1), (1, x2buf, part2)):
            for way in range(2):
                for k in range(6):
                    gather_copy(buf, phase, way, k).wait_send()
                scatter_own(part, phase, way).wait_send()
                for k in range(2):
                    scatter_far(part, phase, way, k).wait_send()
                    scatter_joined(phase, way, k).wait_send()
        for copy in (*stat_copies, small_copy, spatial_copy):
            copy.wait_send()
        sent = (
            *[(valw.at[c, pl.ds(0, 960)], valw.at[c, pl.ds(0, 1024)])] * 2,
            *[(dmw.at[c, pl.ds(0, 960)], dmw.at[c, pl.ds(0, 1024)])] * 2,
            *[(we.at[c, pl.ds(0, 960)], we.at[c, pl.ds(0, 1024)])] * 2,
            *[(wr.at[pl.ds(0, 15), pl.ds(0, 512)], wr.at[:, pl.ds(0, 512)])] * 2,
        )
        for index, (torus, across) in enumerate(sent):
            rcopy(torus, torus, w_send.at[index], w_recv_d2d.at[index], sib).wait_send()
            rcopy(across, across, w_send_d2d.at[index], w_recv_d2d.at[index], sib).wait_send()


def layer(*args):
    (
        tokens,
        mixer_gain,
        direct_weight,
        direct_scale,
        value_weight,
        value_scale,
        value_gain,
        value_shift,
        spatial_weight,
        spatial_bias,
        merge_weight,
        merge_scale,
        channel_gain,
        expand_weight,
        expand_scale,
        reduce_weight,
        reduce_scale,
    ) = args
    operands = (
        tokens,
        mixer_gain.reshape(16, 128),
        direct_weight,
        direct_scale.reshape(1, CW),
        value_weight,
        value_scale.reshape(1, CW),
        value_gain.reshape(1, CW),
        value_shift.reshape(1, CW),
        spatial_weight,
        spatial_bias,
        merge_weight,
        merge_scale.reshape(1, 128),
        channel_gain.reshape(16, 128),
        expand_weight,
        expand_scale.reshape(1, HW),
        reduce_weight,
        reduce_scale.reshape(1, 128),
    )
    vmem = pl.BlockSpec(memory_space=pltpu.VMEM)
    dma = pltpu.SemaphoreType.DMA
    return pl.pallas_call(
        kernel,
        out_shape=jax.ShapeDtypeStruct((R, D), BF16),
        in_specs=[pl.BlockSpec(memory_space=pl.ANY)] * 17,
        out_specs=vmem,
        scratch_shapes=[
            *(pltpu.VMEM(operand.shape, operand.dtype) for operand in operands[1:]),
            pltpu.VMEM((2, D, 128), BF16),
            pltpu.VMEM((2, D, 256), BF16),
            pltpu.VMEM((2, D, HW), BF16),
            pltpu.VMEM((16, 2 * HW, 128), BF16),
            pltpu.VMEM((4 * R, D), BF16),
            pltpu.VMEM((4 * R, D), BF16),
            pltpu.VMEM((4 * R, D), BF16),
            pltpu.VMEM((4 * R, D), BF16),
            pltpu.VMEM((2, 2, 64, D), BF16),
            pltpu.VMEM((2, 2, R, D), BF16),
            pltpu.VMEM((2, 2, 64, D), BF16),
            pltpu.VMEM((4 * R, D), BF16),
            pltpu.VMEM((4 * R, 256), F32),
            pltpu.VMEM((4 * R, 256), F32),
            pltpu.VMEM((4 * R, 256), BF16),
            pltpu.VMEM((4 * R, 128), F32),
            pltpu.VMEM((4, 4, 8, 128), F32),
            pltpu.VMEM((2, 8, 128), F32),
            pltpu.VMEM((2, 2, 128, 128), BF16),
            pltpu.VMEM((2, 128, 128), F32),
            dma((17,)),
            dma((2, 2, 6)),
            dma((2, 2, 6)),
            dma((2, 2, 5)),
            dma((2, 2, 5)),
            dma((3,)),
            dma((3,)),
            dma((2,)),
            dma((2,)),
            dma((8,)),
            dma((8,)),
            dma((8, 4)),
            dma((8, 4, 4)),
            dma((8,)),
        ],
        compiler_params=pltpu.CompilerParams(
            collective_id=0, has_side_effects=True, vmem_limit_bytes=60 * 1024 * 1024
        ),
        name="layer",
    )(*operands)


def solution(mesh):
    finer = Mesh(mesh.devices.reshape(2, 4, 4, 4, 2), AXES)
    in_specs = (
        P(AXES, None),
        P(),
        P(FS, TP),
        P(TP),
        P(FS, TP),
        P(TP),
        P(TP),
        P(TP),
        P(TP, None, None),
        P(TP, None),
        P(TP, FS),
        P(FS),
        P(),
        P(FS, TP),
        P(TP),
        P(TP, FS),
        P(FS),
    )
    return jax.shard_map(layer, mesh=finer, in_specs=in_specs, out_specs=P(AXES, None), check_vma=False)
```

time: 111 us -> 95.6 us (0.86)
  Pallas kernels: 109 us -> 93.6 us
    pallas_call x1, Pallas kernels: 109 us -> 93.6 us  [layer(): pl.pallas_call(kernel, out_shape=jax.ShapeDtypeStruct((R, D), BF16), in_s...]
where the time goes in v2:
time: 95.6 us; the launch traced here: 95.4 us
  Pallas kernels  93.6 us (98%)
  local copies, waits for them, and re-layouts  1.88 us (2%)
    pallas_call x1, Pallas kernels, layer(): pl.pallas_call(kernel, out_shape=jax.ShapeDtypeStruct((R, D), BF16), in_s...  93.6 us

profile of v2, /device:TPU:1, one launch (start us, length us, event | category | flops | bytes accessed | tf_op | source)
XLA Modules:
  0.0 95.4 jit_solution(1767279289449880138)
XLA Ops:
  0.0 93.6 %layer.1 = bf16[128,2048]{1,0:T(8,128)(2,1)} custom-call(bf16[128,2048]{1,0:T(8,128)(2,1)} %tokens.1, f32[16,128]{1,0:T(8,128)} %bitcast.9, f32[128,128]{1,0:T(8,128)} %direct_weight_hbm.1, f32[1,128]{1,0:T(1,128)} %bitcast.12, f32[128,128]{1,0:T(8,128)} %value_weight_hbm.1, f32[1,128]{1,0:T(1,128)} %bitcast.13, f32[1,128]{1,0:T(1,128)} %bitcast.14, ...), custom_call_target="tpu_custom_call" | custom-call | tf_op jit(solution)/shard_map/layer/pallas_call | solution.py:726
  93.6 1.9 %copy.19 = bf16[128,2048]{1,0:T(8,128)(2,1)} copy(bf16[128,2048]{1,0:T(8,128)(2,1)} %layer.1) | data formatting | bytes 1048576

commit v3 on v2

v3 whole, which is shorter than its diff:
```python
import functools

import jax
import jax.numpy as jnp
from jax import lax
from jax.experimental import pallas as pl
from jax.experimental.pallas import tpu as pltpu
from jax.sharding import Mesh
from jax.sharding import PartitionSpec as P

AXES = ("zh", "zl", "x", "y", "c")
FS = ("zl", "x")
TP = ("y", "c")
EPS = 1e-6
MESH = pl.DeviceIdType.MESH
F32 = jnp.float32
BF16 = jnp.bfloat16

D = 2048
R = 128
CW = 128
HW = 1024
BRANCH = 1024
SN, SP, SF, SO = 0, 1, 2, 3
CHUNK = 32


def gelu(u):
    return jax.nn.gelu(u, approximate=True)


class Gather:
    def __init__(self, view, span, a, b, pa, pb, sib, send, send_d2d, recv, recv_d2d):
        self.view, self.span = view, span
        self.a, self.b, self.pa, self.pb, self.sib = a, b, pa, pb, sib
        self.send, self.send_d2d, self.recv, self.recv_d2d = send, send_d2d, recv, recv_d2d

    def item(self, da, db, half=None):
        return self.view(lax.rem(self.pa + 4 - da, 4), lax.rem(self.pb + 4 - db, 4), half)

    def copy(self, ref, stage, to):
        return pltpu.make_async_remote_copy(
            src_ref=ref,
            dst_ref=ref,
            send_sem=self.send,
            recv_sem=self.recv.at[stage],
            device_id=to,
            device_id_type=MESH,
        )

    def landed(self, stage, count):
        self.copy(self.span(count), stage, self.sib).wait_recv()

    def along_b(self, da, stage):
        for k in range(2):
            self.copy(self.item(da, 0), stage, self.b[k]).start()

    def across(self, da, db):
        ref = self.item(da, db)
        pltpu.make_async_remote_copy(
            src_ref=ref,
            dst_ref=ref,
            send_sem=self.send_d2d,
            recv_sem=self.recv_d2d,
            device_id=self.sib,
            device_id_type=MESH,
        ).start()

    def on_b(self, da, stage):
        for k in range(2):
            db = (1, 3)[k]
            self.copy(self.item(da, db, k), stage, self.b[k]).start()
            self.across(da, db)

    def wave0(self):
        for k in range(2):
            self.copy(self.item(0, 0), 0, self.a[k]).start()
        self.along_b(0, 1)
        self.across(0, 0)

    def wave1(self):
        self.landed(0, 2)
        for k in range(2):
            da = (1, 3)[k]
            self.copy(self.item(da, 0, k), 2, self.a[k]).start()
            self.along_b(da, 3)
            self.across(da, 0)
        self.landed(1, 2)
        self.on_b(0, 4)

    def wave2(self):
        self.landed(2, 1)
        self.along_b(2, 5)
        self.across(2, 0)
        self.landed(3, 4)
        self.on_b(1, 6)
        self.on_b(3, 6)
        self.landed(4, 1)
        self.across(0, 2)

    def wave3(self):
        self.landed(5, 2)
        self.on_b(2, 7)
        self.landed(6, 2)
        self.across(1, 2)
        self.across(3, 2)

    def wave4(self):
        self.landed(7, 1)
        self.across(2, 2)


def kernel(
    tokens,
    mixer_gain_hbm,
    direct_weight_hbm,
    direct_scale_hbm,
    value_weight_hbm,
    value_scale_hbm,
    value_gain_hbm,
    value_shift_hbm,
    spatial_weight_hbm,
    spatial_bias_hbm,
    merge_weight_hbm,
    merge_scale_hbm,
    channel_gain_hbm,
    expand_weight_hbm,
    expand_scale_hbm,
    reduce_weight_hbm,
    reduce_scale_hbm,
    out,
    mixer_gain,
    direct_weight,
    direct_scale,
    value_weight,
    value_scale,
    value_gain,
    value_shift,
    spatial_weight,
    spatial_bias,
    merge_weight,
    merge_scale,
    channel_gain,
    expand_weight,
    expand_scale,
    reduce_weight,
    reduce_scale,
    valw,
    dmw,
    we,
    wr,
    xbuf,
    x2buf,
    part1,
    part2,
    rel,
    near,
    mrg,
    hbuf,
    dbuf,
    vbuf,
    gbuf,
    rbuf,
    stat,
    small,
    swb,
    bias,
    result,
    in_sem,
    out_sem,
    ag_send,
    ag_recv,
    rs_send,
    rs_recv,
    st_send,
    st_recv,
    sm_send,
    sm_recv,
    w_send,
    w_send_d2d,
    w_recv,
    w_recv_d2d,
):
    zh, zl, x, y, c = (lax.axis_index(name) for name in AXES)
    z = zh * 4 + zl
    fs = zl * 4 + x
    other = 1 - c
    scope = jax.named_scope

    def at_z(w):
        w = lax.rem(w, 8)
        return {"zh": lax.div(w, 4), "zl": lax.rem(w, 4)}

    xs = ({"x": lax.rem(x + 1, 4)}, {"x": lax.rem(x + 3, 4)})
    zs = (at_z(z + 1), at_z(z + 7))
    ynext, yprev, yfar = ({"y": lax.rem(y + k, 4)} for k in (1, 3, 2))
    sib = {"c": other}

    barrier = pltpu.get_barrier_semaphore()
    for to in (*xs, *zs, ynext, yprev, yfar, sib):
        pl.semaphore_signal(barrier, inc=1, device_id=to, device_id_type=MESH)

    inputs = [
        pltpu.make_async_copy(src, dst, in_sem.at[k])
        for k, (src, dst) in enumerate(
            (
                (tokens, xbuf.at[pl.ds(SO * R, R)]),
                (mixer_gain_hbm, mixer_gain),
                (direct_weight_hbm, direct_weight),
                (direct_scale_hbm, direct_scale),
                (value_weight_hbm, value_weight),
                (value_scale_hbm, value_scale),
                (merge_weight_hbm, merge_weight),
                (merge_scale_hbm, merge_scale),
                (channel_gain_hbm, channel_gain),
                (expand_weight_hbm, expand_weight),
                (expand_scale_hbm, expand_scale),
                (reduce_weight_hbm, reduce_weight),
                (reduce_scale_hbm, reduce_scale),
                (value_gain_hbm, value_gain),
                (value_shift_hbm, value_shift),
                (spatial_bias_hbm, spatial_bias),
                (spatial_weight_hbm, spatial_weight),
            )
        )
    ]
    for copy in inputs:
        copy.start()

    def rcopy(src, dst, ssem, rsem, to):
        return pltpu.make_async_remote_copy(
            src_ref=src, dst_ref=dst, send_sem=ssem, recv_sem=rsem, device_id=to, device_id_type=MESH
        )

    def gather_copy(buf, phase, way, k):
        if k < 4:
            src = buf.at[pl.ds(SO * R + CHUNK * k, CHUNK)]
            dst = buf.at[pl.ds((SP, SN)[way] * R + CHUNK * k, CHUNK)]
            stage = k - 2 * way if k // 2 == way else 2
        else:
            row = 64 * way + CHUNK * (k - 4)
            src = buf.at[pl.ds((SP, SN)[way] * R + row, CHUNK)]
            dst = buf.at[pl.ds(SF * R + row, CHUNK)]
            stage = 3
        return rcopy(src, dst, ag_send.at[phase], ag_recv.at[phase, stage], (ynext, yprev)[way])

    def gather_landed(buf, phase, stage, chunks):
        ref = buf.at[pl.ds(0, chunks * CHUNK)]
        rcopy(ref, ref, ag_send.at[phase], ag_recv.at[phase, stage], sib).wait_recv()

    def gather_pass_on(buf, phase, k):
        gather_landed(buf, phase, k, 2)
        for way in range(2):
            gather_copy(buf, phase, way, 4 + k).start()

    def gather_near(buf, phase):
        gather_landed(buf, phase, 2, 4)

    def gather_far(buf, phase):
        gather_landed(buf, phase, 3, 4)

    def scatter_copy(src, dst, phase, way, stage):
        return rcopy(src, dst, rs_send.at[phase], rs_recv.at[phase, stage], (ynext, yprev)[way])

    def scatter_landed(part, phase, stage, rows):
        ref = part.at[pl.ds(0, rows)]
        rcopy(ref, ref, rs_send.at[phase], rs_recv.at[phase, stage], sib).wait_recv()

    def scatter_own(part, phase):
        for way in range(2):
            src = part.at[pl.ds((SN, SP)[way] * R + 64 * (1 - way), 64)]
            scatter_copy(src, near.at[phase, way, pl.ds(64 * (1 - way), 64)], phase, way, 0).start()

    def scatter_far(part, phase):
        for k in range(2):
            for way in range(2):
                row = CHUNK * k
                src = part.at[pl.ds(SF * R + 64 * way + row, CHUNK)]
                scatter_copy(src, rel.at[phase, way, pl.ds(row, CHUNK)], phase, way, 1 + k).start()

    def scatter_join(part, phase, k):
        scatter_landed(part, phase, 1 + k, 2 * CHUNK)
        for way in range(2):
            row = CHUNK * k
            mine = part[pl.ds((SN, SP)[way] * R + 64 * way + row, CHUNK), :].astype(F32)
            came = rel[phase, way, pl.ds(row, CHUNK), :].astype(F32)
            joined = mrg.at[phase, way, pl.ds(row, CHUNK)]
            joined[...] = (mine + came).astype(BF16)
            scatter_copy(
                joined, near.at[phase, way, pl.ds(64 * way + row, CHUNK)], phase, way, 3 + k
            ).start()

    def scatter_finish(part, phase, base, done, k):
        if k == 0:
            scatter_landed(part, phase, 0, 128)
        scatter_landed(part, phase, 3 + k, 2 * CHUNK)
        for way in range(2):
            row = 64 * way + CHUNK * k
            total = part[pl.ds(SO * R + row, CHUNK), :].astype(F32)
            total = total + near[phase, 0, pl.ds(row, CHUNK), :].astype(F32)
            total = total + near[phase, 1, pl.ds(row, CHUNK), :].astype(F32)
            mine = base[pl.ds(SO * R + row, CHUNK), :].astype(F32)
            done(row, (mine + total).astype(BF16))

    def view_rows(ref, low):
        def view(pz, px, half):
            row = (pz * 4 + px) * 128 + low
            if half is None:
                return ref.at[c, pl.ds(pl.multiple_of(row, 64), 64)]
            return ref.at[c, pl.ds(pl.multiple_of(row + 32 * half, 32), 32)]

        return view

    def span_rows(ref):
        return lambda count: ref.at[c, pl.ds(0, 64 * count)]

    def view_reduce(low):
        def view(pz, px, half):
            row = c * HW + low
            if half is None:
                return wr.at[pz * 4 + px, pl.ds(pl.multiple_of(row, 256), 256)]
            return wr.at[pz * 4 + px, pl.ds(pl.multiple_of(row + 128 * half, 128), 128)]

        return view

    def span_reduce(count):
        return wr.at[pl.ds(0, count), pl.ds(0, 256)]

    def weight(index, view, span, x_first):
        if x_first:
            a, b, pa, pb, turned = xs, zs, x, zl, lambda p, q, h: view(q, p, h)
        else:
            a, b, pa, pb, turned = zs, xs, zl, x, view
        return Gather(
            turned,
            span,
            a,
            b,
            pa,
            pb,
            sib,
            w_send.at[index],
            w_send_d2d.at[index],
            w_recv.at[index],
            w_recv_d2d.at[index],
        )

    class Pair:
        def __init__(self, index, low, high, span):
            self.index, self.span = index, span
            self.halves = (weight(index, low, span, True), weight(index + 1, high, span, False))

        def wave(self, k):
            for half in self.halves:
                getattr(half, f"wave{k}")()

        def shared(self):
            for half in self.halves:
                ref = self.span(16)
                rcopy(ref, ref, half.send_d2d, half.recv_d2d, sib).wait_recv()

        def sent(self):
            for half in self.halves:
                ref = self.span(15)
                rcopy(ref, ref, half.send, half.recv_d2d, sib).wait_send()
                ref = self.span(16)
                rcopy(ref, ref, half.send_d2d, half.recv_d2d, sib).wait_send()

    value_blocks = Pair(0, view_rows(valw, 0), view_rows(valw, 64), span_rows(valw))
    dm_blocks = Pair(2, view_rows(dmw, 0), view_rows(dmw, 64), span_rows(dmw))
    expand_blocks = Pair(4, view_rows(we, 0), view_rows(we, 64), span_rows(we))
    reduce_low = Pair(6, view_reduce(0), view_reduce(256), span_reduce)
    reduce_high = Pair(8, view_reduce(512), view_reduce(768), span_reduce)

    def column(row):
        return jnp.transpose(jnp.broadcast_to(row, (128, 128)))

    with scope("wait_tokens"):
        inputs[0].wait()
    with scope("wait_barrier"):
        pl.semaphore_wait(barrier, 8)
    for k in range(4):
        for way in range(2):
            gather_copy(xbuf, 0, way, (k + 2 * way) % 4).start()
    with scope("wait_mix"):
        for copy in inputs[1:8]:
            copy.wait()

    fs_row = pl.ds(pl.multiple_of(fs * 128, 128), 128)
    gain = column(mixer_gain[pl.ds(fs, 1), :])
    valw[c, fs_row, :] = (value_weight[...] * gain * value_scale[...]).astype(BF16)
    dmw[c, fs_row, 0:128] = (direct_weight[...] * gain * direct_scale[...]).astype(BF16)
    dmw[c, fs_row, 128:256] = (merge_weight[...] * merge_scale[...]).astype(BF16)
    value_blocks.wave(0)
    dm_blocks.wave(0)
    for copy in inputs[8:]:
        copy.wait()
    gain = column(channel_gain[pl.ds(fs, 1), :])
    for k in range(8):
        lanes = slice(k * 128, (k + 1) * 128)
        we[c, fs_row, lanes] = (expand_weight[:, lanes] * gain * expand_scale[:, lanes]).astype(BF16)
    for k in range(8):
        rows = pl.ds(pl.multiple_of(c * HW + k * 128, 128), 128)
        wr[fs, rows, :] = (reduce_weight[k * 128 : (k + 1) * 128, :] * reduce_scale[...]).astype(BF16)
    small[c, 0:1, :] = value_gain[...]
    small[c, 1:2, :] = value_shift[...]
    small[c, 2:4, :] = spatial_bias[...]
    small[c, 4:8, :] = jnp.zeros((4, 128), F32)
    swb[c] = spatial_weight[...]
    small_copy = rcopy(small.at[c], small.at[c], sm_send.at[0], sm_recv.at[0], sib)
    spatial_copy = rcopy(spatial_weight, swb.at[c], sm_send.at[1], sm_recv.at[1], sib)
    small_copy.start()
    spatial_copy.start()

    def row_scales(buf, start, count):
        @pl.loop(0, count // 32)
        def _(i):
            rows = pl.ds(pl.multiple_of(start + i * 32, 32), 32)
            floats = buf[rows, :].astype(F32)
            power = jnp.mean(floats * floats, axis=-1, keepdims=True)
            rbuf[rows, :] = jnp.broadcast_to(lax.rsqrt(power + EPS), (32, 128))

    lane = lax.broadcasted_iota(jnp.int32, (128, 128), 1)
    block_of = {SP: lax.rem(y + 3, 4), SN: lax.rem(y + 1, 4), SF: lax.rem(y + 2, 4), SO: y}

    def project(slots):
        start, count = slots[0] * R, len(slots) * R
        rows = pl.ds(start, count)
        weights = jnp.concatenate([valw[0], valw[1]], axis=1)
        value = jnp.dot(xbuf[rows, :], weights, preferred_element_type=F32)
        scale = rbuf[rows, :]
        vbuf[rows, :] = gelu(value * jnp.concatenate([scale, scale], axis=1))
        for slot in slots:
            v = vbuf[pl.ds(slot * R, R), :]
            total = jnp.sum(v, axis=1, keepdims=True)
            squares = jnp.sum(v * v, axis=1, keepdims=True)
            tile = jnp.where(lane == 0, total, jnp.where(lane == 1, squares, 0.0))
            stat[0, block_of[slot]] = jnp.transpose(tile)[0:8, :]

    def project_direct():
        weights = jnp.concatenate([dmw[0, :, 0:128], dmw[1, :, 0:128]], axis=1)

        @pl.loop(0, 2)
        def _(i):
            rows = pl.ds(pl.multiple_of(i * 256, 256), 256)
            direct = jnp.dot(xbuf[rows, :], weights, preferred_element_type=F32)
            scale = rbuf[rows, :]
            dbuf[rows, :] = gelu(direct * jnp.concatenate([scale, scale], axis=1))

    def mixing(slots):
        for slot in slots:
            rows = pl.ds(slot * R, R)
            block = block_of[slot]
            sums = stat[0, block] + stat[1, block] + stat[2, block] + stat[3, block]
            tile = jnp.transpose(jnp.concatenate([sums] * 16, axis=0))
            mean = tile[:, 0:1] / BRANCH
            var = tile[:, 1:2] / BRANCH - mean * mean
            inv = lax.rsqrt(var + EPS)
            for k in range(2):
                lanes = slice(k * 128, (k + 1) * 128)
                v = vbuf[rows, lanes]
                g = ((v - mean) * inv * small[k, 0:1, :] + small[k, 1:2, :]).astype(BF16)
                low = jnp.dot(swb[k, 0], g, preferred_element_type=F32)
                high = jnp.dot(swb[k, 1], g, preferred_element_type=F32)
                mixed = jnp.where(lane < 64, low, high) + bias[k]
                gbuf[rows, lanes] = (dbuf[rows, lanes] * mixed).astype(BF16)
        rows = pl.ds(slots[0] * R, len(slots) * R)

        @pl.loop(0, 2)
        def _(j):
            weights = jnp.concatenate(
                [
                    jnp.concatenate(
                        [
                            dmw[k, pl.ds(pl.multiple_of(j * 1024 + i * 128, 128), 128), 128:256]
                            for i in range(8)
                        ],
                        axis=1,
                    )
                    for k in range(2)
                ],
                axis=0,
            )
            product = jnp.dot(gbuf[rows, :], weights, preferred_element_type=F32)
            part1[rows, pl.ds(pl.multiple_of(j * 1024, 1024), 1024)] = product.astype(BF16)

    def gathered_rows(ref, pieces):
        loaded = [ref[pl.ds(start, count), :] for start, count in pieces]
        return loaded[0] if len(loaded) == 1 else jnp.concatenate(loaded, axis=0)

    def store_rows(ref, pieces, cols, values):
        at = 0
        for start, count in pieces:
            ref[pl.ds(start, count), cols] = values[at : at + count, :]
            at += count

    def feed_up(pieces):
        for start, count in pieces:
            row_scales(x2buf, start, count)

        @pl.loop(0, 2)
        def _(j):
            upper = jnp.dot(gathered_rows(x2buf, pieces), we[j], preferred_element_type=F32)
            upper = upper * jnp.concatenate([gathered_rows(rbuf, pieces)] * 8, axis=1)
            hidden = jnp.square(jnp.maximum(upper, 0.0)).astype(BF16)
            store_rows(hbuf, pieces, pl.ds(pl.multiple_of(j * HW, HW), HW), hidden)

    def feed_down(pieces):
        @pl.loop(0, 2)
        def _(j):
            weights = jnp.concatenate([wr[8 * j + i] for i in range(8)], axis=1)
            product = jnp.dot(gathered_rows(hbuf, pieces), weights, preferred_element_type=F32)
            store_rows(part2, pieces, pl.ds(pl.multiple_of(j * 1024, 1024), 1024), product.astype(BF16))

    row_scales(xbuf, SO * R, R)
    with scope("v_w1"):
        value_blocks.wave(1)
    with scope("dm_w1"):
        dm_blocks.wave(1)
    expand_blocks.halves[0].wave0()
    with scope("v_w2"):
        value_blocks.wave(2)
    with scope("pass1_0"):
        gather_pass_on(xbuf, 0, 0)
    with scope("dm_w2"):
        dm_blocks.wave(2)
    with scope("v_w3"):
        value_blocks.wave(3)
    expand_blocks.halves[1].wave0()
    with scope("pass1_1"):
        gather_pass_on(xbuf, 0, 1)
    with scope("dm_w3"):
        dm_blocks.wave(3)
    with scope("near1"):
        gather_near(xbuf, 0)
    with scope("scales_near"):
        row_scales(xbuf, 0, 2 * R)
    with scope("v_w4"):
        value_blocks.wave(4)
    with scope("v_d2d"):
        value_blocks.shared()
    with scope("project_own"):
        project((SO,))
    with scope("e_w1"):
        expand_blocks.wave(1)
    with scope("project_near"):
        project((SN, SP))
    with scope("dm_w4"):
        dm_blocks.wave(4)
    with scope("far1"):
        gather_far(xbuf, 0)
    with scope("project_far"):
        row_scales(xbuf, SF * R, R)
        project((SF,))
    stat_copies = [
        rcopy(stat.at[0], stat.at[k + 1], st_send.at[0], st_recv.at[0], to)
        for k, to in enumerate((ynext, yprev, yfar))
    ]
    for copy in stat_copies:
        copy.start()
    reduce_low.wave(0)
    reduce_high.wave(0)
    with scope("dm_d2d"):
        dm_blocks.shared()
    with scope("direct"):
        project_direct()
        rcopy(small.at[other], small.at[other], sm_send.at[0], sm_recv.at[0], sib).wait_recv()
        rcopy(swb.at[other], swb.at[other], sm_send.at[1], sm_recv.at[1], sib).wait_recv()
        for k in range(2):
            rows = jnp.concatenate(
                [jnp.broadcast_to(small[k, 2 + g : 3 + g, :], (64, 128)) for g in range(2)], axis=0
            )
            bias[k] = jnp.transpose(rows)
    with scope("wait_stats"):
        all_stats = stat.at[pl.ds(1, 3)]
        rcopy(all_stats, all_stats, st_send.at[0], st_recv.at[0], sib).wait_recv()
    with scope("mixing_near"):
        mixing((SN, SP))
    scatter_own(part1, 0)
    with scope("mixing_far"):
        mixing((SF,))
    scatter_far(part1, 0)
    with scope("mixing_own"):
        mixing((SO,))
    with scope("e_w2"):
        expand_blocks.wave(2)
    with scope("r0_w1"):
        reduce_low.wave(1)
    with scope("join1_0"):
        scatter_join(part1, 0, 0)
    with scope("join1_1"):
        scatter_join(part1, 0, 1)
    with scope("e_w3"):
        expand_blocks.wave(3)
    with scope("r1_w1"):
        reduce_high.wave(1)

    def middle_done(row, value):
        x2buf[pl.ds(SO * R + row, CHUNK), :] = value

    with scope("finish1_0"):
        scatter_finish(part1, 0, xbuf, middle_done, 0)
    for way in range(2):
        gather_copy(x2buf, 1, way, 2 * way).start()
    with scope("r0_w2"):
        reduce_low.wave(2)
    with scope("finish1_1"):
        scatter_finish(part1, 0, xbuf, middle_done, 1)
    for way in range(2):
        gather_copy(x2buf, 1, way, 2 * way + 1).start()
    with scope("e_w4"):
        expand_blocks.wave(4)
    with scope("pass2_0"):
        gather_pass_on(x2buf, 1, 0)
    with scope("r1_w2"):
        reduce_high.wave(2)
    with scope("pass2_1"):
        gather_pass_on(x2buf, 1, 1)
    for k in range(2):
        for way in range(2):
            gather_copy(x2buf, 1, way, 2 * (1 - way) + k).start()

    outer, inner = ((64, 128),), ((0, 64), (192, 64))
    far, own = ((SF * R, R),), ((SO * R, R),)
    with scope("e_d2d"):
        expand_blocks.shared()
    with scope("up_outer"):
        feed_up(outer)
    with scope("r0_w3"):
        reduce_low.wave(3)
    with scope("r1_w3"):
        reduce_high.wave(3)
    with scope("up_own"):
        feed_up(own)
    with scope("r0_w4"):
        reduce_low.wave(4)
    with scope("r1_w4"):
        reduce_high.wave(4)
    with scope("r_d2d"):
        reduce_low.shared()
        reduce_high.shared()
    with scope("down_outer"):
        feed_down(outer)
    scatter_own(part2, 1)
    with scope("far2"):
        gather_far(x2buf, 1)
    with scope("feed_far"):
        feed_up(far)
        feed_down(far)
    scatter_far(part2, 1)
    with scope("near2"):
        gather_near(x2buf, 1)
    with scope("feed_inner"):
        feed_up(inner)
        feed_down(inner)
    with scope("down_own"):
        feed_down(own)
    with scope("join2_0"):
        scatter_join(part2, 1, 0)
    with scope("join2_1"):
        scatter_join(part2, 1, 1)

    def result_done(row, value):
        result[pl.ds(row, CHUNK), :] = value

    def result_copy(row):
        rows = pl.ds(row, CHUNK)
        return pltpu.make_async_copy(result.at[rows], out.at[rows], out_sem.at[row // CHUNK])

    for k in range(2):
        with scope(f"finish2_{k}"):
            scatter_finish(part2, 1, x2buf, result_done, k)
        for way in range(2):
            result_copy(64 * way + CHUNK * k).start()

    with scope("drain"):
        for phase, buf, part in ((0, xbuf, part1), (1, x2buf, part2)):
            ref = buf.at[pl.ds(0, 12 * CHUNK)]
            rcopy(ref, ref, ag_send.at[phase], ag_recv.at[phase, 0], sib).wait_send()
            ref = part.at[pl.ds(0, 12 * CHUNK)]
            rcopy(ref, ref, rs_send.at[phase], rs_recv.at[phase, 0], sib).wait_send()
        rcopy(all_stats, all_stats, st_send.at[0], st_recv.at[0], sib).wait_send()
        for copy in (small_copy, spatial_copy):
            copy.wait_send()
        for blocks in (value_blocks, dm_blocks, expand_blocks, reduce_low, reduce_high):
            blocks.sent()
        for k in range(4):
            result_copy(CHUNK * k).wait()


def layer(*args):
    (
        tokens,
        mixer_gain,
        direct_weight,
        direct_scale,
        value_weight,
        value_scale,
        value_gain,
        value_shift,
        spatial_weight,
        spatial_bias,
        merge_weight,
        merge_scale,
        channel_gain,
        expand_weight,
        expand_scale,
        reduce_weight,
        reduce_scale,
    ) = args
    operands = (
        tokens,
        mixer_gain.reshape(16, 128),
        direct_weight,
        direct_scale.reshape(1, CW),
        value_weight,
        value_scale.reshape(1, CW),
        value_gain.reshape(1, CW),
        value_shift.reshape(1, CW),
        spatial_weight,
        spatial_bias,
        merge_weight,
        merge_scale.reshape(1, 128),
        channel_gain.reshape(16, 128),
        expand_weight,
        expand_scale.reshape(1, HW),
        reduce_weight,
        reduce_scale.reshape(1, 128),
    )
    dma = pltpu.SemaphoreType.DMA
    return pl.pallas_call(
        kernel,
        out_shape=jax.ShapeDtypeStruct((R, D), BF16),
        in_specs=[pl.BlockSpec(memory_space=pl.ANY)] * 17,
        out_specs=pl.BlockSpec(memory_space=pl.ANY),
        scratch_shapes=[
            *(pltpu.VMEM(operand.shape, operand.dtype) for operand in operands[1:]),
            pltpu.VMEM((2, D, 128), BF16),
            pltpu.VMEM((2, D, 256), BF16),
            pltpu.VMEM((2, D, HW), BF16),
            pltpu.VMEM((16, 2 * HW, 128), BF16),
            pltpu.VMEM((4 * R, D), BF16),
            pltpu.VMEM((4 * R, D), BF16),
            pltpu.VMEM((4 * R, D), BF16),
            pltpu.VMEM((4 * R, D), BF16),
            pltpu.VMEM((2, 2, 64, D), BF16),
            pltpu.VMEM((2, 2, R, D), BF16),
            pltpu.VMEM((2, 2, 64, D), BF16),
            pltpu.VMEM((4 * R, D), BF16),
            pltpu.VMEM((4 * R, 256), F32),
            pltpu.VMEM((4 * R, 256), F32),
            pltpu.VMEM((4 * R, 256), BF16),
            pltpu.VMEM((4 * R, 128), F32),
            pltpu.VMEM((4, 4, 8, 128), F32),
            pltpu.VMEM((2, 8, 128), F32),
            pltpu.VMEM((2, 2, 128, 128), BF16),
            pltpu.VMEM((2, 128, 128), F32),
            pltpu.VMEM((R, D), BF16),
            dma((17,)),
            dma((4,)),
            dma((2,)),
            dma((2, 4)),
            dma((2,)),
            dma((2, 5)),
            dma((1,)),
            dma((1,)),
            dma((2,)),
            dma((2,)),
            dma((10,)),
            dma((10,)),
            dma((10, 8)),
            dma((10,)),
        ],
        compiler_params=pltpu.CompilerParams(
            collective_id=0, has_side_effects=True, vmem_limit_bytes=60 * 1024 * 1024
        ),
        name="layer",
    )(*operands)


def solution(mesh):
    finer = Mesh(mesh.devices.reshape(2, 4, 4, 4, 2), AXES)
    in_specs = (
        P(AXES, None),
        P(),
        P(FS, TP),
        P(TP),
        P(FS, TP),
        P(TP),
        P(TP),
        P(TP),
        P(TP, None, None),
        P(TP, None),
        P(TP, FS),
        P(FS),
        P(),
        P(FS, TP),
        P(TP),
        P(TP, FS),
        P(FS),
    )
    return jax.shard_map(layer, mesh=finer, in_specs=in_specs, out_specs=P(AXES, None), check_vma=False)
```

time: 95.6 us -> 93.3 us (0.976)
  Pallas kernels: 93.6 us -> 91.3 us
    pallas_call x1, Pallas kernels: 93.6 us -> 91.3 us  [layer(): pl.pallas_call(kernel, out_shape=jax.ShapeDtypeStruct((R, D), BF16), in_s...]
where the time goes in v3:
time: 93.3 us; the launch traced here: 93.2 us
  Pallas kernels  91.3 us (98%)
  local copies, waits for them, and re-layouts  1.88 us (2%)
    pallas_call x1, Pallas kernels, layer(): pl.pallas_call(kernel, out_shape=jax.ShapeDtypeStruct((R, D), BF16), in_s...  91.3 us
    unnamed x1, local copies, waits for them, and re-layouts  1.88 us

profile of v3, /device:TPU:1, one launch (start us, length us, event | category | flops | bytes accessed | tf_op | source)
XLA Modules:
  0.0 93.2 jit_solution(1123366762092702615)
XLA Ops:
  0.0 91.3 %layer.1 = bf16[128,2048]{1,0:T(8,128)(2,1)} custom-call(bf16[128,2048]{1,0:T(8,128)(2,1)} %tokens.1, f32[16,128]{1,0:T(8,128)} %bitcast.9, f32[128,128]{1,0:T(8,128)} %direct_weight_hbm.1, f32[1,128]{1,0:T(1,128)} %bitcast.12, f32[128,128]{1,0:T(8,128)} %value_weight_hbm.1, f32[1,128]{1,0:T(1,128)} %bitcast.13, f32[1,128]{1,0:T(1,128)} %bitcast.14, ...), custom_call_target="tpu_custom_call" | custom-call | tf_op jit(solution)/shard_map/layer/pallas_call | solution.py:731
  91.3 1.9 %copy.19 = bf16[128,2048]{1,0:T(8,128)(2,1)} copy(bf16[128,2048]{1,0:T(8,128)(2,1)} %layer.1) | data formatting | bytes 1048576

commit v4 on v3

--- a/solution.py
+++ b/solution.py
@@ -27,6 +27,10 @@
 
 def gelu(u):
     return jax.nn.gelu(u, approximate=True)
+
+
+FIRST = ((0, 0), (1, 0), (3, 0), (0, 1), (0, 3), (1, 1), (1, 3), (3, 1))
+LAST = ((3, 3), (2, 0), (0, 2), (2, 1), (2, 3), (1, 2), (3, 2), (2, 2))
 
 
 class Gather:
@@ -61,7 +65,7 @@
             src_ref=ref,
             dst_ref=ref,
             send_sem=self.send_d2d,
-            recv_sem=self.recv_d2d,
+            recv_sem=self.recv_d2d.at[0 if (da, db) in FIRST else 1],
             device_id=self.sib,
             device_id_type=MESH,
         ).start()
@@ -153,15 +157,19 @@
     x2buf,
     part1,
     part2,
-    rel,
-    near,
-    mrg,
+    rel1,
+    near1,
+    mrg1,
+    rel2,
+    near2,
+    mrg2,
     hbuf,
     dbuf,
     vbuf,
     gbuf,
     rbuf,
     stat,
+    totals,
     small,
     swb,
     bias,
@@ -259,48 +267,54 @@
     def gather_far(buf, phase):
         gather_landed(buf, phase, 3, 4)
 
-    def scatter_copy(src, dst, phase, way, stage):
-        return rcopy(src, dst, rs_send.at[phase], rs_recv.at[phase, stage], (ynext, yprev)[way])
-
-    def scatter_landed(part, phase, stage, rows):
-        ref = part.at[pl.ds(0, rows)]
-        rcopy(ref, ref, rs_send.at[phase], rs_recv.at[phase, stage], sib).wait_recv()
-
-    def scatter_own(part, phase):
-        for way in range(2):
-            src = part.at[pl.ds((SN, SP)[way] * R + 64 * (1 - way), 64)]
-            scatter_copy(src, near.at[phase, way, pl.ds(64 * (1 - way), 64)], phase, way, 0).start()
-
-    def scatter_far(part, phase):
-        for k in range(2):
+    class Scatter:
+        def __init__(self, stage, part, near, rel, mrg):
+            self.stage, self.part, self.near, self.rel, self.mrg = stage, part, near, rel, mrg
+
+        def copy(self, src, dst, way, k):
+            return rcopy(
+                src, dst, rs_send.at[self.stage], rs_recv.at[self.stage, k], (ynext, yprev)[way]
+            )
+
+        def landed(self, k, rows):
+            ref = self.part.at[pl.ds(0, rows)]
+            rcopy(ref, ref, rs_send.at[self.stage], rs_recv.at[self.stage, k], sib).wait_recv()
+
+        def own(self):
+            for way in range(2):
+                row = 64 * (1 - way)
+                src = self.part.at[pl.ds((SN, SP)[way] * R + row, 64)]
+                self.copy(src, self.near.at[way, pl.ds(row, 64)], way, 0).start()
+
+        def far(self):
+            for k in range(2):
+                for way in range(2):
+                    row = CHUNK * k
+                    src = self.part.at[pl.ds(SF * R + 64 * way + row, CHUNK)]
+                    self.copy(src, self.rel.at[way, pl.ds(row, CHUNK)], way, 1 + k).start()
+
+        def join(self, k):
+            self.landed(1 + k, 2 * CHUNK)
             for way in range(2):
                 row = CHUNK * k
-                src = part.at[pl.ds(SF * R + 64 * way + row, CHUNK)]
-                scatter_copy(src, rel.at[phase, way, pl.ds(row, CHUNK)], phase, way, 1 + k).start()
-
-    def scatter_join(part, phase, k):
-        scatter_landed(part, phase, 1 + k, 2 * CHUNK)
-        for way in range(2):
-            row = CHUNK * k
-            mine = part[pl.ds((SN, SP)[way] * R + 64 * way + row, CHUNK), :].astype(F32)
-            came = rel[phase, way, pl.ds(row, CHUNK), :].astype(F32)
-            joined = mrg.at[phase, way, pl.ds(row, CHUNK)]
-            joined[...] = (mine + came).astype(BF16)
-            scatter_copy(
-                joined, near.at[phase, way, pl.ds(64 * way + row, CHUNK)], phase, way, 3 + k
-            ).start()
-
-    def scatter_finish(part, phase, base, done, k):
-        if k == 0:
-            scatter_landed(part, phase, 0, 128)
-        scatter_landed(part, phase, 3 + k, 2 * CHUNK)
-        for way in range(2):
-            row = 64 * way + CHUNK * k
-            total = part[pl.ds(SO * R + row, CHUNK), :].astype(F32)
-            total = total + near[phase, 0, pl.ds(row, CHUNK), :].astype(F32)
-            total = total + near[phase, 1, pl.ds(row, CHUNK), :].astype(F32)
-            mine = base[pl.ds(SO * R + row, CHUNK), :].astype(F32)
-            done(row, (mine + total).astype(BF16))
+                mine = self.part[pl.ds((SN, SP)[way] * R + 64 * way + row, CHUNK), :].astype(F32)
+                came = self.rel[way, pl.ds(row, CHUNK), :].astype(F32)
+                joined = self.mrg.at[way, pl.ds(row, CHUNK)]
+                joined[...] = (mine + came).astype(BF16)
+                self.copy(joined, self.near.at[way, pl.ds(64 * way + row, CHUNK)], way, 3 + k).start()
+
+        def finish(self, k, done):
+            if k == 0:
+                self.landed(0, 128)
+            self.landed(3 + k, 2 * CHUNK)
+            for way in range(2):
+                row = 64 * way + CHUNK * k
+                total = self.part[pl.ds(SO * R + row, CHUNK), :].astype(F32)
+                total = total + self.near[0, pl.ds(row, CHUNK), :].astype(F32)
+                done(row, total + self.near[1, pl.ds(row, CHUNK), :].astype(F32))
+
+    mixer_sums = Scatter(0, part1, near1, rel1, mrg1)
+    ff_sums = [Scatter(1 + g, part2.at[g], near2.at[g], rel2.at[g], mrg2.at[g]) for g in range(2)]
 
     def view_rows(ref, low):
         def view(pz, px, half):
@@ -354,17 +368,17 @@
             for half in self.halves:
                 getattr(half, f"wave{k}")()
 
-        def shared(self):
+        def shared(self, group):
             for half in self.halves:
-                ref = self.span(16)
-                rcopy(ref, ref, half.send_d2d, half.recv_d2d, sib).wait_recv()
+                ref = self.span(8)
+                rcopy(ref, ref, half.send_d2d, half.recv_d2d.at[group], sib).wait_recv()
 
         def sent(self):
             for half in self.halves:
                 ref = self.span(15)
-                rcopy(ref, ref, half.send, half.recv_d2d, sib).wait_send()
+                rcopy(ref, ref, half.send, half.recv_d2d.at[0], sib).wait_send()
                 ref = self.span(16)
-                rcopy(ref, ref, half.send_d2d, half.recv_d2d, sib).wait_send()
+                rcopy(ref, ref, half.send_d2d, half.recv_d2d.at[0], sib).wait_send()
 
     value_blocks = Pair(0, view_rows(valw, 0), view_rows(valw, 64), span_rows(valw))
     dm_blocks = Pair(2, view_rows(dmw, 0), view_rows(dmw, 64), span_rows(dmw))
@@ -379,9 +393,13 @@
         inputs[0].wait()
     with scope("wait_barrier"):
         pl.semaphore_wait(barrier, 8)
-    for k in range(4):
-        for way in range(2):
-            gather_copy(xbuf, 0, way, (k + 2 * way) % 4).start()
+
+    def send_tokens():
+        for k in range(4):
+            for way in range(2):
+                gather_copy(xbuf, 0, way, (k + 2 * way) % 4).start()
+
+    pl.when(c == 1)(send_tokens)
     with scope("wait_mix"):
         for copy in inputs[1:8]:
             copy.wait()
@@ -435,7 +453,9 @@
             total = jnp.sum(v, axis=1, keepdims=True)
             squares = jnp.sum(v * v, axis=1, keepdims=True)
             tile = jnp.where(lane == 0, total, jnp.where(lane == 1, squares, 0.0))
-            stat[0, block_of[slot]] = jnp.transpose(tile)[0:8, :]
+            sums = jnp.transpose(tile)
+            stat[0, pl.ds(block_of[slot], 1), :] = sums[0:1, :]
+            stat[0, pl.ds(4 + block_of[slot], 1), :] = sums[1:2, :]
 
     def project_direct():
         weights = jnp.concatenate([dmw[0, :, 0:128], dmw[1, :, 0:128]], axis=1)
@@ -451,10 +471,8 @@
         for slot in slots:
             rows = pl.ds(slot * R, R)
             block = block_of[slot]
-            sums = stat[0, block] + stat[1, block] + stat[2, block] + stat[3, block]
-            tile = jnp.transpose(jnp.concatenate([sums] * 16, axis=0))
-            mean = tile[:, 0:1] / BRANCH
-            var = tile[:, 1:2] / BRANCH - mean * mean
+            mean = column(totals[pl.ds(block, 1), :]) / BRANCH
+            var = column(totals[pl.ds(4 + block, 1), :]) / BRANCH - mean * mean
             inv = lax.rsqrt(var + EPS)
             for k in range(2):
                 lanes = slice(k * 128, (k + 1) * 128)
@@ -505,52 +523,85 @@
             hidden = jnp.square(jnp.maximum(upper, 0.0)).astype(BF16)
             store_rows(hbuf, pieces, pl.ds(pl.multiple_of(j * HW, HW), HW), hidden)
 
-    def feed_down(pieces):
-        @pl.loop(0, 2)
-        def _(j):
-            weights = jnp.concatenate([wr[8 * j + i] for i in range(8)], axis=1)
-            product = jnp.dot(gathered_rows(hbuf, pieces), weights, preferred_element_type=F32)
-            store_rows(part2, pieces, pl.ds(pl.multiple_of(j * 1024, 1024), 1024), product.astype(BF16))
+    def shard_of(dx, dz):
+        return lax.rem(zl + 4 - dz, 4) * 4 + lax.rem(x + 4 - dx, 4)
+
+    columns = [[shard_of(*offsets) for offsets in group] for group in (FIRST, LAST)]
+
+    def feed_down(pieces, g):
+        weights = jnp.concatenate([wr[shard] for shard in columns[g]], axis=1)
+        product = jnp.dot(gathered_rows(hbuf, pieces), weights, preferred_element_type=F32)
+        store_rows(part2.at[g], pieces, slice(None), product.astype(BF16))
 
     row_scales(xbuf, SO * R, R)
     with scope("v_w1"):
         value_blocks.wave(1)
     with scope("dm_w1"):
         dm_blocks.wave(1)
-    expand_blocks.halves[0].wave0()
+
+    @pl.when(c == 1)
+    def _():
+        gather_pass_on(xbuf, 0, 0)
+        gather_pass_on(xbuf, 0, 1)
+
     with scope("v_w2"):
         value_blocks.wave(2)
-    with scope("pass1_0"):
-        gather_pass_on(xbuf, 0, 0)
+    pl.when(c == 0)(send_tokens)
     with scope("dm_w2"):
         dm_blocks.wave(2)
     with scope("v_w3"):
         value_blocks.wave(3)
-    expand_blocks.halves[1].wave0()
-    with scope("pass1_1"):
-        gather_pass_on(xbuf, 0, 1)
+    expand_blocks.wave(0)
+
+    @pl.when(c == 1)
+    def _():
+        with scope("scales_1"):
+            gather_near(xbuf, 0)
+            gather_far(xbuf, 0)
+            row_scales(xbuf, 0, 3 * R)
+
+    @pl.when(c == 0)
+    def _():
+        with scope("pass1_0"):
+            gather_pass_on(xbuf, 0, 0)
+
+    with scope("v_w4"):
+        value_blocks.wave(4)
     with scope("dm_w3"):
         dm_blocks.wave(3)
-    with scope("near1"):
-        gather_near(xbuf, 0)
-    with scope("scales_near"):
-        row_scales(xbuf, 0, 2 * R)
-    with scope("v_w4"):
-        value_blocks.wave(4)
+    reduce_low.wave(0)
+
+    @pl.when(c == 0)
+    def _():
+        with scope("pass1_1"):
+            gather_pass_on(xbuf, 0, 1)
+
     with scope("v_d2d"):
-        value_blocks.shared()
+        value_blocks.shared(0)
+        value_blocks.shared(1)
     with scope("project_own"):
         project((SO,))
-    with scope("e_w1"):
-        expand_blocks.wave(1)
+
+    @pl.when(c == 0)
+    def _():
+        with scope("scales_0"):
+            gather_near(xbuf, 0)
+            row_scales(xbuf, 0, 2 * R)
+
     with scope("project_near"):
         project((SN, SP))
     with scope("dm_w4"):
         dm_blocks.wave(4)
-    with scope("far1"):
-        gather_far(xbuf, 0)
+
+    @pl.when(c == 0)
+    def _():
+        with scope("e_w1_0"):
+            expand_blocks.wave(1)
+        with scope("far1"):
+            gather_far(xbuf, 0)
+            row_scales(xbuf, 2 * R, R)
+
     with scope("project_far"):
-        row_scales(xbuf, SF * R, R)
         project((SF,))
     stat_copies = [
         rcopy(stat.at[0], stat.at[k + 1], st_send.at[0], st_recv.at[0], to)
@@ -558,10 +609,16 @@
     ]
     for copy in stat_copies:
         copy.start()
-    reduce_low.wave(0)
+
+    @pl.when(c == 1)
+    def _():
+        with scope("e_w1_1"):
+            expand_blocks.wave(1)
+
     reduce_high.wave(0)
     with scope("dm_d2d"):
-        dm_blocks.shared()
+        dm_blocks.shared(0)
+        dm_blocks.shared(1)
     with scope("direct"):
         project_direct()
         rcopy(small.at[other], small.at[other], sm_send.at[0], sm_recv.at[0], sib).wait_recv()
@@ -574,12 +631,13 @@
     with scope("wait_stats"):
         all_stats = stat.at[pl.ds(1, 3)]
         rcopy(all_stats, all_stats, st_send.at[0], st_recv.at[0], sib).wait_recv()
+        totals[...] = stat[0] + stat[1] + stat[2] + stat[3]
     with scope("mixing_near"):
         mixing((SN, SP))
-    scatter_own(part1, 0)
+    mixer_sums.own()
     with scope("mixing_far"):
         mixing((SF,))
-    scatter_far(part1, 0)
+    mixer_sums.far()
     with scope("mixing_own"):
         mixing((SO,))
     with scope("e_w2"):
@@ -587,25 +645,26 @@
     with scope("r0_w1"):
         reduce_low.wave(1)
     with scope("join1_0"):
-        scatter_join(part1, 0, 0)
+        mixer_sums.join(0)
     with scope("join1_1"):
-        scatter_join(part1, 0, 1)
+        mixer_sums.join(1)
     with scope("e_w3"):
         expand_blocks.wave(3)
     with scope("r1_w1"):
         reduce_high.wave(1)
 
-    def middle_done(row, value):
-        x2buf[pl.ds(SO * R + row, CHUNK), :] = value
+    def middle_done(row, total):
+        rows = pl.ds(SO * R + row, CHUNK)
+        x2buf[rows, :] = (xbuf[rows, :].astype(F32) + total).astype(BF16)
 
     with scope("finish1_0"):
-        scatter_finish(part1, 0, xbuf, middle_done, 0)
+        mixer_sums.finish(0, middle_done)
     for way in range(2):
         gather_copy(x2buf, 1, way, 2 * way).start()
     with scope("r0_w2"):
         reduce_low.wave(2)
     with scope("finish1_1"):
-        scatter_finish(part1, 0, xbuf, middle_done, 1)
+        mixer_sums.finish(1, middle_done)
     for way in range(2):
         gather_copy(x2buf, 1, way, 2 * way + 1).start()
     with scope("e_w4"):
@@ -623,62 +682,86 @@
     outer, inner = ((64, 128),), ((0, 64), (192, 64))
     far, own = ((SF * R, R),), ((SO * R, R),)
     with scope("e_d2d"):
-        expand_blocks.shared()
+        expand_blocks.shared(0)
+        expand_blocks.shared(1)
     with scope("up_outer"):
         feed_up(outer)
     with scope("r0_w3"):
         reduce_low.wave(3)
+    with scope("r_d2d_0"):
+        reduce_low.shared(0)
+        reduce_high.shared(0)
+    with scope("down_outer_0"):
+        feed_down(outer, 0)
+    ff_sums[0].own()
     with scope("r1_w3"):
         reduce_high.wave(3)
-    with scope("up_own"):
-        feed_up(own)
+    with scope("far2"):
+        gather_far(x2buf, 1)
+    with scope("feed_far_0"):
+        feed_up(far)
+        feed_down(far, 0)
+    ff_sums[0].far()
     with scope("r0_w4"):
         reduce_low.wave(4)
     with scope("r1_w4"):
         reduce_high.wave(4)
-    with scope("r_d2d"):
-        reduce_low.shared()
-        reduce_high.shared()
-    with scope("down_outer"):
-        feed_down(outer)
-    scatter_own(part2, 1)
-    with scope("far2"):
-        gather_far(x2buf, 1)
-    with scope("feed_far"):
-        feed_up(far)
-        feed_down(far)
-    scatter_far(part2, 1)
+    with scope("r_d2d_1"):
+        reduce_low.shared(1)
+        reduce_high.shared(1)
+    with scope("down_outer_1"):
+        feed_down(outer, 1)
+    ff_sums[1].own()
+    with scope("down_far_1"):
+        feed_down(far, 1)
+    ff_sums[1].far()
     with scope("near2"):
         gather_near(x2buf, 1)
-    with scope("feed_inner"):
+    with scope("feed_inner_0"):
         feed_up(inner)
-        feed_down(inner)
-    with scope("down_own"):
-        feed_down(own)
+        feed_down(inner, 0)
     with scope("join2_0"):
-        scatter_join(part2, 1, 0)
+        ff_sums[0].join(0)
+        ff_sums[0].join(1)
+    with scope("feed_inner_1"):
+        feed_down(inner, 1)
+    with scope("feed_own"):
+        feed_up(own)
+        feed_down(own, 0)
+        feed_down(own, 1)
     with scope("join2_1"):
-        scatter_join(part2, 1, 1)
-
-    def result_done(row, value):
-        result[pl.ds(row, CHUNK), :] = value
+        ff_sums[1].join(0)
+        ff_sums[1].join(1)
+
+    def result_done(g):
+        def done(row, total):
+            for p, shard in enumerate(columns[g]):
+                lanes = pl.ds(pl.multiple_of(shard * 128, 128), 128)
+                mine = x2buf[pl.ds(SO * R + row, CHUNK), lanes].astype(F32)
+                added = mine + total[:, p * 128 : (p + 1) * 128]
+                result[pl.ds(row, CHUNK), lanes] = added.astype(BF16)
+
+        return done
 
     def result_copy(row):
         rows = pl.ds(row, CHUNK)
         return pltpu.make_async_copy(result.at[rows], out.at[rows], out_sem.at[row // CHUNK])
 
-    for k in range(2):
-        with scope(f"finish2_{k}"):
-            scatter_finish(part2, 1, x2buf, result_done, k)
-        for way in range(2):
-            result_copy(64 * way + CHUNK * k).start()
+    for g in range(2):
+        for k in range(2):
+            with scope(f"finish2_{g}_{k}"):
+                ff_sums[g].finish(k, result_done(g))
+            if g == 1:
+                for way in range(2):
+                    result_copy(64 * way + CHUNK * k).start()
 
     with scope("drain"):
-        for phase, buf, part in ((0, xbuf, part1), (1, x2buf, part2)):
+        for phase, buf in ((0, xbuf), (1, x2buf)):
             ref = buf.at[pl.ds(0, 12 * CHUNK)]
             rcopy(ref, ref, ag_send.at[phase], ag_recv.at[phase, 0], sib).wait_send()
-            ref = part.at[pl.ds(0, 12 * CHUNK)]
-            rcopy(ref, ref, rs_send.at[phase], rs_recv.at[phase, 0], sib).wait_send()
+        for sums in (mixer_sums, *ff_sums):
+            ref = sums.part.at[pl.ds(0, 12 * CHUNK)]
+            rcopy(ref, ref, rs_send.at[sums.stage], rs_recv.at[sums.stage, 0], sib).wait_send()
         rcopy(all_stats, all_stats, st_send.at[0], st_recv.at[0], sib).wait_send()
         for copy in (small_copy, spatial_copy):
             copy.wait_send()
@@ -742,16 +825,20 @@
             pltpu.VMEM((4 * R, D), BF16),
             pltpu.VMEM((4 * R, D), BF16),
             pltpu.VMEM((4 * R, D), BF16),
-            pltpu.VMEM((4 * R, D), BF16),
-            pltpu.VMEM((2, 2, 64, D), BF16),
-            pltpu.VMEM((2, 2, R, D), BF16),
-            pltpu.VMEM((2, 2, 64, D), BF16),
+            pltpu.VMEM((2, 4 * R, D // 2), BF16),
+            pltpu.VMEM((2, 64, D), BF16),
+            pltpu.VMEM((2, R, D), BF16),
+            pltpu.VMEM((2, 64, D), BF16),
+            pltpu.VMEM((2, 2, 64, D // 2), BF16),
+            pltpu.VMEM((2, 2, R, D // 2), BF16),
+            pltpu.VMEM((2, 2, 64, D // 2), BF16),
             pltpu.VMEM((4 * R, D), BF16),
             pltpu.VMEM((4 * R, 256), F32),
             pltpu.VMEM((4 * R, 256), F32),
             pltpu.VMEM((4 * R, 256), BF16),
             pltpu.VMEM((4 * R, 128), F32),
-            pltpu.VMEM((4, 4, 8, 128), F32),
+            pltpu.VMEM((4, 8, 128), F32),
+            pltpu.VMEM((8, 128), F32),
             pltpu.VMEM((2, 8, 128), F32),
             pltpu.VMEM((2, 2, 128, 128), BF16),
             pltpu.VMEM((2, 128, 128), F32),
@@ -760,8 +847,8 @@
             dma((4,)),
             dma((2,)),
             dma((2, 4)),
-            dma((2,)),
-            dma((2, 5)),
+            dma((3,)),
+            dma((3, 5)),
             dma((1,)),
             dma((1,)),
             dma((2,)),
@@ -769,7 +856,7 @@
             dma((10,)),
             dma((10,)),
             dma((10, 8)),
-            dma((10,)),
+            dma((10, 2)),
         ],
         compiler_params=pltpu.CompilerParams(
             collective_id=0, has_side_effects=True, vmem_limit_bytes=60 * 1024 * 1024

time: 93.3 us -> 89.2 us (0.956)
  Pallas kernels: 91.3 us -> 87.1 us
    pallas_call x1, Pallas kernels: 91.3 us -> 87.1 us  [layer(): pl.pallas_call(kernel, out_shape=jax.ShapeDtypeStruct((R, D), BF16), in_s...]
where the time goes in v4:
time: 89.2 us; the launch traced here: 89 us
  Pallas kernels  87.1 us (98%)
  local copies, waits for them, and re-layouts  1.88 us (2%)
    pallas_call x1, Pallas kernels, layer(): pl.pallas_call(kernel, out_shape=jax.ShapeDtypeStruct((R, D), BF16), in_s...  87.1 us
    unnamed x1, local copies, waits for them, and re-layouts  1.88 us

profile of v4, /device:TPU:1, one launch (start us, length us, event | category | flops | bytes accessed | tf_op | source)
XLA Modules:
  0.0 89.0 jit_solution(3629313650781580303)
XLA Ops:
  0.0 87.1 %layer.1 = bf16[128,2048]{1,0:T(8,128)(2,1)} custom-call(bf16[128,2048]{1,0:T(8,128)(2,1)} %tokens.1, f32[16,128]{1,0:T(8,128)} %bitcast.9, f32[128,128]{1,0:T(8,128)} %direct_weight_hbm.1, f32[1,128]{1,0:T(1,128)} %bitcast.12, f32[128,128]{1,0:T(8,128)} %value_weight_hbm.1, f32[1,128]{1,0:T(1,128)} %bitcast.13, f32[1,128]{1,0:T(1,128)} %bitcast.14, ...), custom_call_target="tpu_custom_call" | custom-call | tf_op jit(solution)/shard_map/layer/pallas_call | solution.py:814
  87.1 1.9 %copy.19 = bf16[128,2048]{1,0:T(8,128)(2,1)} copy(bf16[128,2048]{1,0:T(8,128)(2,1)} %layer.1) | data formatting | bytes 1048576

commit v5 on v4

--- a/solution.py
+++ b/solution.py
@@ -112,6 +112,37 @@
     def wave4(self):
         self.landed(7, 1)
         self.across(2, 2)
+
+
+class DirectGather(Gather):
+    def wave0(self):
+        for k in range(2):
+            self.copy(self.item(0, 0), 0, self.a[k]).start()
+        for k in range(2):
+            self.copy(self.item(0, 0, k), 0, self.far_a[k]).start()
+        self.along_b(0, 1)
+        self.across(0, 0)
+
+    def wave1(self):
+        self.landed(0, 3)
+        for da in (1, 3, 2):
+            self.along_b(da, 2)
+        self.landed(1, 2)
+        self.on_b(0, 3)
+        for da in (1, 3, 2):
+            self.across(da, 0)
+
+    def wave2(self):
+        self.landed(2, 6)
+        for da in (1, 3, 2):
+            self.on_b(da, 4)
+        self.landed(3, 1)
+        self.across(0, 2)
+
+    def wave3(self):
+        self.landed(4, 3)
+        for da in (1, 3, 2):
+            self.across(da, 2)
 
 
 def kernel(
@@ -174,6 +205,7 @@
     swb,
     bias,
     result,
+    base,
     in_sem,
     out_sem,
     ag_send,
@@ -201,11 +233,13 @@
 
     xs = ({"x": lax.rem(x + 1, 4)}, {"x": lax.rem(x + 3, 4)})
     zs = (at_z(z + 1), at_z(z + 7))
+    xs_far = ({"x": lax.rem(x + 2, 4)},) * 2
+    zs_far = (at_z(z + 2), at_z(z + 6))
     ynext, yprev, yfar = ({"y": lax.rem(y + k, 4)} for k in (1, 3, 2))
     sib = {"c": other}
 
     barrier = pltpu.get_barrier_semaphore()
-    for to in (*xs, *zs, ynext, yprev, yfar, sib):
+    for to in (*xs, xs_far[0], *zs, *zs_far, ynext, yprev, yfar, sib):
         pl.semaphore_signal(barrier, inc=1, device_id=to, device_id_type=MESH)
 
     inputs = [
@@ -268,8 +302,9 @@
         gather_landed(buf, phase, 3, 4)
 
     class Scatter:
-        def __init__(self, stage, part, near, rel, mrg):
+        def __init__(self, stage, part, near, rel, mrg, mine):
             self.stage, self.part, self.near, self.rel, self.mrg = stage, part, near, rel, mrg
+            self.mine = mine
 
         def copy(self, src, dst, way, k):
             return rcopy(
@@ -309,12 +344,23 @@
             self.landed(3 + k, 2 * CHUNK)
             for way in range(2):
                 row = 64 * way + CHUNK * k
-                total = self.part[pl.ds(SO * R + row, CHUNK), :].astype(F32)
-                total = total + self.near[0, pl.ds(row, CHUNK), :].astype(F32)
+                total = self.mine(row) + self.near[0, pl.ds(row, CHUNK), :].astype(F32)
                 done(row, total + self.near[1, pl.ds(row, CHUNK), :].astype(F32))
 
-    mixer_sums = Scatter(0, part1, near1, rel1, mrg1)
-    ff_sums = [Scatter(1 + g, part2.at[g], near2.at[g], rel2.at[g], mrg2.at[g]) for g in range(2)]
+    mixer_sums = Scatter(
+        0, part1, near1, rel1, mrg1, lambda row: part1[pl.ds(SO * R + row, CHUNK), :].astype(F32)
+    )
+    ff_sums = [
+        Scatter(
+            1 + g,
+            part2.at[g],
+            near2.at[g],
+            rel2.at[g],
+            mrg2.at[g],
+            lambda row, g=g: base[g, pl.ds(row, CHUNK), :],
+        )
+        for g in range(2)
+    ]
 
     def view_rows(ref, low):
         def view(pz, px, half):
@@ -340,12 +386,12 @@
     def span_reduce(count):
         return wr.at[pl.ds(0, count), pl.ds(0, 256)]
 
-    def weight(index, view, span, x_first):
+    def weight(index, view, span, x_first, form=Gather):
         if x_first:
             a, b, pa, pb, turned = xs, zs, x, zl, lambda p, q, h: view(q, p, h)
         else:
             a, b, pa, pb, turned = zs, xs, zl, x, view
-        return Gather(
+        blocks = form(
             turned,
             span,
             a,
@@ -358,11 +404,16 @@
             w_recv.at[index],
             w_recv_d2d.at[index],
         )
+        blocks.far_a = xs_far if x_first else zs_far
+        return blocks
 
     class Pair:
-        def __init__(self, index, low, high, span):
+        def __init__(self, index, low, high, span, form=Gather):
             self.index, self.span = index, span
-            self.halves = (weight(index, low, span, True), weight(index + 1, high, span, False))
+            self.halves = (
+                weight(index, low, span, True, form),
+                weight(index + 1, high, span, False, form),
+            )
 
         def wave(self, k):
             for half in self.halves:
@@ -380,8 +431,8 @@
                 ref = self.span(16)
                 rcopy(ref, ref, half.send_d2d, half.recv_d2d.at[0], sib).wait_send()
 
-    value_blocks = Pair(0, view_rows(valw, 0), view_rows(valw, 64), span_rows(valw))
-    dm_blocks = Pair(2, view_rows(dmw, 0), view_rows(dmw, 64), span_rows(dmw))
+    value_blocks = Pair(0, view_rows(valw, 0), view_rows(valw, 64), span_rows(valw), DirectGather)
+    dm_blocks = Pair(2, view_rows(dmw, 0), view_rows(dmw, 64), span_rows(dmw), DirectGather)
     expand_blocks = Pair(4, view_rows(we, 0), view_rows(we, 64), span_rows(we))
     reduce_low = Pair(6, view_reduce(0), view_reduce(256), span_reduce)
     reduce_high = Pair(8, view_reduce(512), view_reduce(768), span_reduce)
@@ -392,7 +443,7 @@
     with scope("wait_tokens"):
         inputs[0].wait()
     with scope("wait_barrier"):
-        pl.semaphore_wait(barrier, 8)
+        pl.semaphore_wait(barrier, 11)
 
     def send_tokens():
         for k in range(4):
@@ -533,11 +584,19 @@
         product = jnp.dot(gathered_rows(hbuf, pieces), weights, preferred_element_type=F32)
         store_rows(part2.at[g], pieces, slice(None), product.astype(BF16))
 
+    def feed_own(g):
+        weights = jnp.concatenate([wr[shard] for shard in columns[g]], axis=1)
+        rows = pl.ds(SO * R, R)
+        middle = [x2buf[rows, pl.ds(pl.multiple_of(shard * 128, 128), 128)] for shard in columns[g]]
+        product = jnp.dot(hbuf[rows, :], weights, preferred_element_type=F32)
+        base[g] = jnp.concatenate(middle, axis=1).astype(F32) + product.astype(BF16).astype(F32)
+
     row_scales(xbuf, SO * R, R)
     with scope("v_w1"):
         value_blocks.wave(1)
     with scope("dm_w1"):
         dm_blocks.wave(1)
+    pl.when(c == 0)(send_tokens)
 
     @pl.when(c == 1)
     def _():
@@ -546,30 +605,30 @@
 
     with scope("v_w2"):
         value_blocks.wave(2)
-    pl.when(c == 0)(send_tokens)
-    with scope("dm_w2"):
-        dm_blocks.wave(2)
-    with scope("v_w3"):
-        value_blocks.wave(3)
-    expand_blocks.wave(0)
+    expand_blocks.halves[0].wave0()
 
     @pl.when(c == 1)
     def _():
         with scope("scales_1"):
             gather_near(xbuf, 0)
-            gather_far(xbuf, 0)
-            row_scales(xbuf, 0, 3 * R)
+            row_scales(xbuf, 0, 2 * R)
 
     @pl.when(c == 0)
     def _():
         with scope("pass1_0"):
             gather_pass_on(xbuf, 0, 0)
 
-    with scope("v_w4"):
-        value_blocks.wave(4)
-    with scope("dm_w3"):
-        dm_blocks.wave(3)
+    with scope("dm_w2"):
+        dm_blocks.wave(2)
+    expand_blocks.halves[1].wave0()
     reduce_low.wave(0)
+    with scope("v_w3"):
+        value_blocks.wave(3)
+
+    @pl.when(c == 1)
+    def _():
+        gather_far(xbuf, 0)
+        row_scales(xbuf, 2 * R, R)
 
     @pl.when(c == 0)
     def _():
@@ -582,19 +641,20 @@
     with scope("project_own"):
         project((SO,))
 
+    @pl.when(c == 1)
+    def _():
+        project((SN, SP))
+
+    with scope("dm_w3"):
+        dm_blocks.wave(3)
+
     @pl.when(c == 0)
     def _():
         with scope("scales_0"):
             gather_near(xbuf, 0)
             row_scales(xbuf, 0, 2 * R)
-
-    with scope("project_near"):
-        project((SN, SP))
-    with scope("dm_w4"):
-        dm_blocks.wave(4)
-
-    @pl.when(c == 0)
-    def _():
+        with scope("project_near"):
+            project((SN, SP))
         with scope("e_w1_0"):
             expand_blocks.wave(1)
         with scope("far1"):
@@ -609,12 +669,6 @@
     ]
     for copy in stat_copies:
         copy.start()
-
-    @pl.when(c == 1)
-    def _():
-        with scope("e_w1_1"):
-            expand_blocks.wave(1)
-
     reduce_high.wave(0)
     with scope("dm_d2d"):
         dm_blocks.shared(0)
@@ -628,6 +682,12 @@
                 [jnp.broadcast_to(small[k, 2 + g : 3 + g, :], (64, 128)) for g in range(2)], axis=0
             )
             bias[k] = jnp.transpose(rows)
+
+    @pl.when(c == 1)
+    def _():
+        with scope("e_w1_1"):
+            expand_blocks.wave(1)
+
     with scope("wait_stats"):
         all_stats = stat.at[pl.ds(1, 3)]
         rcopy(all_stats, all_stats, st_send.at[0], st_recv.at[0], sib).wait_recv()
@@ -640,12 +700,22 @@
     mixer_sums.far()
     with scope("mixing_own"):
         mixing((SO,))
+
+    @pl.when(c == 1)
+    def _():
+        with scope("join1_0_1"):
+            mixer_sums.join(0)
+
     with scope("e_w2"):
         expand_blocks.wave(2)
     with scope("r0_w1"):
         reduce_low.wave(1)
-    with scope("join1_0"):
-        mixer_sums.join(0)
+
+    @pl.when(c == 0)
+    def _():
+        with scope("join1_0_0"):
+            mixer_sums.join(0)
+
     with scope("join1_1"):
         mixer_sums.join(1)
     with scope("e_w3"):
@@ -661,12 +731,12 @@
         mixer_sums.finish(0, middle_done)
     for way in range(2):
         gather_copy(x2buf, 1, way, 2 * way).start()
-    with scope("r0_w2"):
-        reduce_low.wave(2)
     with scope("finish1_1"):
         mixer_sums.finish(1, middle_done)
     for way in range(2):
         gather_copy(x2buf, 1, way, 2 * way + 1).start()
+    with scope("r0_w2"):
+        reduce_low.wave(2)
     with scope("e_w4"):
         expand_blocks.wave(4)
     with scope("pass2_0"):
@@ -696,16 +766,20 @@
     ff_sums[0].own()
     with scope("r1_w3"):
         reduce_high.wave(3)
+    with scope("up_own"):
+        feed_up(own)
     with scope("far2"):
         gather_far(x2buf, 1)
+    with scope("r0_w4"):
+        reduce_low.wave(4)
+    with scope("r1_w4"):
+        reduce_high.wave(4)
     with scope("feed_far_0"):
         feed_up(far)
         feed_down(far, 0)
     ff_sums[0].far()
-    with scope("r0_w4"):
-        reduce_low.wave(4)
-    with scope("r1_w4"):
-        reduce_high.wave(4)
+    with scope("down_own_0"):
+        feed_own(0)
     with scope("r_d2d_1"):
         reduce_low.shared(1)
         reduce_high.shared(1)
@@ -725,35 +799,29 @@
         ff_sums[0].join(1)
     with scope("feed_inner_1"):
         feed_down(inner, 1)
-    with scope("feed_own"):
-        feed_up(own)
-        feed_down(own, 0)
-        feed_down(own, 1)
-    with scope("join2_1"):
+    with scope("join2_1_0"):
         ff_sums[1].join(0)
+    with scope("join2_1_1"):
         ff_sums[1].join(1)
+    with scope("down_own_1"):
+        feed_own(1)
 
     def result_done(g):
         def done(row, total):
-            for p, shard in enumerate(columns[g]):
-                lanes = pl.ds(pl.multiple_of(shard * 128, 128), 128)
-                mine = x2buf[pl.ds(SO * R + row, CHUNK), lanes].astype(F32)
-                added = mine + total[:, p * 128 : (p + 1) * 128]
-                result[pl.ds(row, CHUNK), lanes] = added.astype(BF16)
+            result[g, pl.ds(row, CHUNK), :] = total.astype(BF16)
 
         return done
-
-    def result_copy(row):
-        rows = pl.ds(row, CHUNK)
-        return pltpu.make_async_copy(result.at[rows], out.at[rows], out_sem.at[row // CHUNK])
 
     for g in range(2):
         for k in range(2):
             with scope(f"finish2_{g}_{k}"):
                 ff_sums[g].finish(k, result_done(g))
-            if g == 1:
-                for way in range(2):
-                    result_copy(64 * way + CHUNK * k).start()
+        for p, shard in enumerate(columns[g]):
+            pltpu.make_async_copy(
+                result.at[g, :, pl.ds(p * 128, 128)],
+                out.at[:, pl.ds(pl.multiple_of(shard * 128, 128), 128)],
+                out_sem.at[0],
+            ).start()
 
     with scope("drain"):
         for phase, buf in ((0, xbuf), (1, x2buf)):
@@ -767,8 +835,7 @@
             copy.wait_send()
         for blocks in (value_blocks, dm_blocks, expand_blocks, reduce_low, reduce_high):
             blocks.sent()
-        for k in range(4):
-            result_copy(CHUNK * k).wait()
+        pltpu.make_async_copy(result, result, out_sem.at[0]).wait()
 
 
 def layer(*args):
@@ -842,9 +909,10 @@
             pltpu.VMEM((2, 8, 128), F32),
             pltpu.VMEM((2, 2, 128, 128), BF16),
             pltpu.VMEM((2, 128, 128), F32),
-            pltpu.VMEM((R, D), BF16),
+            pltpu.VMEM((2, R, D // 2), BF16),
+            pltpu.VMEM((2, R, D // 2), F32),
             dma((17,)),
-            dma((4,)),
+            dma((1,)),
             dma((2,)),
             dma((2, 4)),
             dma((3,)),

time: 89.2 us -> 88.3 us (0.990)
  no operation moved by 1% of the time
where the time goes in v5:
time: 88.3 us; the launch traced here: 88.2 us
  Pallas kernels  86.3 us (98%)
  local copies, waits for them, and re-layouts  1.88 us (2%)
    pallas_call x1, Pallas kernels, layer(): pl.pallas_call(kernel, out_shape=jax.ShapeDtypeStruct((R, D), BF16), in_s...  86.3 us
    unnamed x1, local copies, waits for them, and re-layouts  1.88 us

profile of v5, /device:TPU:1, one launch (start us, length us, event | category | flops | bytes accessed | tf_op | source)
XLA Modules:
  0.0 88.2 jit_solution(2728930746513178716)
XLA Ops:
  0.0 86.3 %layer.1 = bf16[128,2048]{1,0:T(8,128)(2,1)} custom-call(bf16[128,2048]{1,0:T(8,128)(2,1)} %tokens.1, f32[16,128]{1,0:T(8,128)} %bitcast.9, f32[128,128]{1,0:T(8,128)} %direct_weight_hbm.1, f32[1,128]{1,0:T(1,128)} %bitcast.12, f32[128,128]{1,0:T(8,128)} %value_weight_hbm.1, f32[1,128]{1,0:T(1,128)} %bitcast.13, f32[1,128]{1,0:T(1,128)} %bitcast.14, ...), custom_call_target="tpu_custom_call" | custom-call | tf_op jit(solution)/shard_map/layer/pallas_call | solution.py:881
  86.3 1.9 %copy.19 = bf16[128,2048]{1,0:T(8,128)(2,1)} copy(bf16[128,2048]{1,0:T(8,128)(2,1)} %layer.1) | data formatting | bytes 1048576

commit v6 on v5

--- a/solution.py
+++ b/solution.py
@@ -204,10 +204,8 @@
     small,
     swb,
     bias,
-    result,
     base,
     in_sem,
-    out_sem,
     ag_send,
     ag_recv,
     rs_send,
@@ -508,15 +506,12 @@
             stat[0, pl.ds(block_of[slot], 1), :] = sums[0:1, :]
             stat[0, pl.ds(4 + block_of[slot], 1), :] = sums[1:2, :]
 
-    def project_direct():
+    def project_direct(start):
         weights = jnp.concatenate([dmw[0, :, 0:128], dmw[1, :, 0:128]], axis=1)
-
-        @pl.loop(0, 2)
-        def _(i):
-            rows = pl.ds(pl.multiple_of(i * 256, 256), 256)
-            direct = jnp.dot(xbuf[rows, :], weights, preferred_element_type=F32)
-            scale = rbuf[rows, :]
-            dbuf[rows, :] = gelu(direct * jnp.concatenate([scale, scale], axis=1))
+        rows = pl.ds(start, 256)
+        direct = jnp.dot(xbuf[rows, :], weights, preferred_element_type=F32)
+        scale = rbuf[rows, :]
+        dbuf[rows, :] = gelu(direct * jnp.concatenate([scale, scale], axis=1))
 
     def mixing(slots):
         for slot in slots:
@@ -605,7 +600,10 @@
 
     with scope("v_w2"):
         value_blocks.wave(2)
-    expand_blocks.halves[0].wave0()
+
+    with scope("dm_w2"):
+        dm_blocks.wave(2)
+    expand_blocks.wave(0)
 
     @pl.when(c == 1)
     def _():
@@ -618,9 +616,6 @@
         with scope("pass1_0"):
             gather_pass_on(xbuf, 0, 0)
 
-    with scope("dm_w2"):
-        dm_blocks.wave(2)
-    expand_blocks.halves[1].wave0()
     reduce_low.wave(0)
     with scope("v_w3"):
         value_blocks.wave(3)
@@ -655,8 +650,6 @@
             row_scales(xbuf, 0, 2 * R)
         with scope("project_near"):
             project((SN, SP))
-        with scope("e_w1_0"):
-            expand_blocks.wave(1)
         with scope("far1"):
             gather_far(xbuf, 0)
             row_scales(xbuf, 2 * R, R)
@@ -669,12 +662,18 @@
     ]
     for copy in stat_copies:
         copy.start()
+
+    @pl.when(c == 0)
+    def _():
+        with scope("e_w1_0"):
+            expand_blocks.wave(1)
+
     reduce_high.wave(0)
     with scope("dm_d2d"):
         dm_blocks.shared(0)
         dm_blocks.shared(1)
     with scope("direct"):
-        project_direct()
+        project_direct(0)
         rcopy(small.at[other], small.at[other], sm_send.at[0], sm_recv.at[0], sib).wait_recv()
         rcopy(swb.at[other], swb.at[other], sm_send.at[1], sm_recv.at[1], sib).wait_recv()
         for k in range(2):
@@ -695,6 +694,7 @@
     with scope("mixing_near"):
         mixing((SN, SP))
     mixer_sums.own()
+    project_direct(256)
     with scope("mixing_far"):
         mixing((SF,))
     mixer_sums.far()
@@ -808,7 +808,10 @@
 
     def result_done(g):
         def done(row, total):
-            result[g, pl.ds(row, CHUNK), :] = total.astype(BF16)
+            total = total.astype(BF16)
+            for p, shard in enumerate(columns[g]):
+                lanes = pl.ds(pl.multiple_of(shard * 128, 128), 128)
+                out[pl.ds(row, CHUNK), lanes] = total[:, p * 128 : (p + 1) * 128]
 
         return done
 
@@ -816,12 +819,6 @@
         for k in range(2):
             with scope(f"finish2_{g}_{k}"):
                 ff_sums[g].finish(k, result_done(g))
-        for p, shard in enumerate(columns[g]):
-            pltpu.make_async_copy(
-                result.at[g, :, pl.ds(p * 128, 128)],
-                out.at[:, pl.ds(pl.multiple_of(shard * 128, 128), 128)],
-                out_sem.at[0],
-            ).start()
 
     with scope("drain"):
         for phase, buf in ((0, xbuf), (1, x2buf)):
@@ -835,7 +832,6 @@
             copy.wait_send()
         for blocks in (value_blocks, dm_blocks, expand_blocks, reduce_low, reduce_high):
             blocks.sent()
-        pltpu.make_async_copy(result, result, out_sem.at[0]).wait()
 
 
 def layer(*args):
@@ -882,7 +878,7 @@
         kernel,
         out_shape=jax.ShapeDtypeStruct((R, D), BF16),
         in_specs=[pl.BlockSpec(memory_space=pl.ANY)] * 17,
-        out_specs=pl.BlockSpec(memory_space=pl.ANY),
+        out_specs=pl.BlockSpec(memory_space=pltpu.VMEM),
         scratch_shapes=[
             *(pltpu.VMEM(operand.shape, operand.dtype) for operand in operands[1:]),
             pltpu.VMEM((2, D, 128), BF16),
@@ -909,10 +905,8 @@
             pltpu.VMEM((2, 8, 128), F32),
             pltpu.VMEM((2, 2, 128, 128), BF16),
             pltpu.VMEM((2, 128, 128), F32),
-            pltpu.VMEM((2, R, D // 2), BF16),
             pltpu.VMEM((2, R, D // 2), F32),
             dma((17,)),
-            dma((1,)),
             dma((2,)),
             dma((2, 4)),
             dma((3,)),
@@ -927,10 +921,10 @@
             dma((10, 2)),
         ],
         compiler_params=pltpu.CompilerParams(
-            collective_id=0, has_side_effects=True, vmem_limit_bytes=60 * 1024 * 1024
+            collective_id=0, has_side_effects=True, vmem_limit_bytes=52 * 1024 * 1024
         ),
         name="layer",
-    )(*operands)
+    )(*(pltpu.with_memory_space_constraint(operand, pltpu.HBM) for operand in operands))
 
 
 def solution(mesh):

time: 88.3 us -> 85 us (0.963)
  Pallas kernels: 86.3 us -> 83.3 us
  local copies, waits for them, and re-layouts: 1.88 us -> 0.8 us
    pallas_call x1, Pallas kernels: 86.3 us -> 83.3 us  [layer(): pl.pallas_call(kernel, out_shape=jax.ShapeDtypeStruct((R, D), BF16), in_s...]
    unnamed x1, local copies, waits for them, and re-layouts: 1.88 us -> 0.8 us
where the time goes in v6:
time: 85 us; the launch traced here: 84.1 us
  Pallas kernels  83.3 us (98%)
    pallas_call x1, Pallas kernels, layer(): pl.pallas_call(kernel, out_shape=jax.ShapeDtypeStruct((R, D), BF16), in_s...  83.3 us

profile of v6, /device:TPU:1, one launch (start us, length us, event | category | flops | bytes accessed | tf_op | source)
XLA Modules:
  0.0 84.1 jit_solution(4581965617713463445)
XLA Ops:
  0.0 83.3 %layer.1 = bf16[128,2048]{1,0:T(8,128)(2,1)S(1)} custom-call(bf16[128,2048]{1,0:T(8,128)(2,1)} %tokens.1, f32[16,128]{1,0:T(8,128)} %bitcast.9, f32[128,128]{1,0:T(8,128)} %direct_weight_hbm.1, f32[1,128]{1,0:T(1,128)} %bitcast.12, f32[128,128]{1,0:T(8,128)} %value_weight_hbm.1, f32[1,128]{1,0:T(1,128)} %bitcast.13, f32[1,128]{1,0:T(1,128)} %bitcast.14, ...), custom_call_target="tpu_custom_call" | custom-call | tf_op jit(solution)/shard_map/layer/pallas_call | solution.py:877
  83.3 0.8 copy.19

commit v7 on v6

--- a/solution.py
+++ b/solution.py
@@ -633,12 +633,16 @@
     with scope("v_d2d"):
         value_blocks.shared(0)
         value_blocks.shared(1)
-    with scope("project_own"):
-        project((SO,))
 
     @pl.when(c == 1)
     def _():
-        project((SN, SP))
+        with scope("project_all"):
+            project((SN, SP, SF, SO))
+
+    @pl.when(c == 0)
+    def _():
+        with scope("project_own"):
+            project((SO,))
 
     with scope("dm_w3"):
         dm_blocks.wave(3)
@@ -653,9 +657,9 @@
         with scope("far1"):
             gather_far(xbuf, 0)
             row_scales(xbuf, 2 * R, R)
-
-    with scope("project_far"):
-        project((SF,))
+        with scope("project_far"):
+            project((SF,))
+
     stat_copies = [
         rcopy(stat.at[0], stat.at[k + 1], st_send.at[0], st_recv.at[0], to)
         for k, to in enumerate((ynext, yprev, yfar))

time: 85 us -> 85 us (level)
  no operation moved by 1% of the time
where the time goes in v7:
time: 85 us; the launch traced here: 83.9 us
  Pallas kernels  83.1 us (98%)
    pallas_call x1, Pallas kernels, layer(): pl.pallas_call(kernel, out_shape=jax.ShapeDtypeStruct((R, D), BF16), in_s...  83.1 us

profile of v7, /device:TPU:1, one launch (start us, length us, event | category | flops | bytes accessed | tf_op | source)
XLA Modules:
  0.0 83.9 jit_solution(7722107028465630637)
XLA Ops:
  0.0 83.1 %layer.1 = bf16[128,2048]{1,0:T(8,128)(2,1)S(1)} custom-call(bf16[128,2048]{1,0:T(8,128)(2,1)} %tokens.1, f32[16,128]{1,0:T(8,128)} %bitcast.9, f32[128,128]{1,0:T(8,128)} %direct_weight_hbm.1, f32[1,128]{1,0:T(1,128)} %bitcast.12, f32[128,128]{1,0:T(8,128)} %value_weight_hbm.1, f32[1,128]{1,0:T(1,128)} %bitcast.13, f32[1,128]{1,0:T(1,128)} %bitcast.14, ...), custom_call_target="tpu_custom_call" | custom-call | tf_op jit(solution)/shard_map/layer/pallas_call | solution.py:881
  83.1 0.8 copy.19
